TPU v7x, 32 devices: a whole 2x2x4 slice. The times are simulated.
32 devices in a mesh: sp: 16 (over z, y, core), tp: 2 (over x).
Axes of the slice: x: 2, y: 2, z: 4, core: 2. Of those that a mesh axis runs over, the one named last changes fastest.
Arguments:
- asking_matrix: bfloat16 [2048, 2048], P('sp', 'tp'), may hold values from -30 to 30
- matching_key_matrix: bfloat16 [2048, 1024], P('sp', 'tp'), may hold values from -30 to 30
- carried_value_matrix: bfloat16 [2048, 1024], P('sp', 'tp'), may hold values from -48 to 48
- silu_switch_argument: bfloat16 [2048, 2048], P('sp', 'tp'), may hold values from -6 to 6
- duality_source_matrix: bfloat16 [2048, 2048], P('sp', 'tp'), may hold values from -6 to 6
- storing_direction_matrix: bfloat16 [2048, 1024], P('sp', 'tp'), may hold values from -6 to 6
- fetching_direction_matrix: bfloat16 [2048, 1024], P('sp', 'tp'), may hold values from -6 to 6
- duality_kernel_coefficients: bfloat16 [5, 2048], P(None, 'tp'), may hold values from -2.5 to 2.5
- storing_kernel_coefficients: bfloat16 [5, 1024], P(None, 'tp'), may hold values from -2.5 to 2.5
- fetching_kernel_coefficients: bfloat16 [5, 1024], P(None, 'tp'), may hold values from -2.5 to 2.5
- raw_increment_lengths: float32 [2, 32, 2048], P(None, 'tp', 'sp'), may hold values from -5.5 to 5.5
- logarithmic_fading_speeds: float32 [2, 32], P(None, 'tp'), may hold values from -16 to -2.9
- token_fading_spikes: float32 [2, 32, 2048], P(None, 'tp', 'sp'), may hold values from -2.1 to 0
- absorber_score_vector: float32 [16], P('tp'), may hold values from 4 to 8
- cluster_scaling_factor: float32 [2048], P('tp'), may hold values from 0.1 to 1.9
- final_mapping_matrix: bfloat16 [2, 2048, 4096], P(None, 'tp', 'sp'), may hold values from -0.09375 to 0.09375
Outputs:
- mixed_out: bfloat16 [2048, 4096], P(('sp', 'tp'))
All inputs are finite; a program needn't handle non-finite values.
Results may differ from a plain program's by a relative error of at most 0.014.
Values may be sent and summed in bfloat16 or wider, within the bound.
A program may use at most 128 MiB of HBM per device.

v0:
```python
import functools

import jax
import jax.numpy as jnp
from jax import lax
from jax.experimental import pallas as pl
from jax.experimental.pallas import tpu as pltpu
from jax.sharding import PartitionSpec as P

HEAD = 128
SSD_HEAD = 64
STATE = 128
CONV = 5
WINDOW = 128
SPAN = 128


ROTARY_BASE = 500000.0
EPSILON = 1e-06


def padded_2(cells, sides, width):
    for axis, dim in sides:
        count = lax.axis_size(axis)
        ends = count - 1
        head = lax.slice_in_dim(cells, 0, width, axis=dim)
        tail = lax.slice_in_dim(cells, cells.shape[dim] - width, cells.shape[dim], axis=dim)
        cells = jnp.concatenate(
            [
                lax.ppermute(tail, axis, [(i, (i + 1) % count) for i in range(ends)]),
                cells,
                lax.ppermute(head, axis, [((i + 1) % count, i) for i in range(ends)]),
            ],
            axis=dim,
        )
    return cells


def clique_of(count):
    return 4 if count % 4 == 0 else (2 if count % 2 == 0 else 1)


def greet(partners):
    barrier = pltpu.get_barrier_semaphore()
    for partner in partners:
        pl.semaphore_signal(
            barrier, inc=1, device_id=partner, device_id_type=pl.DeviceIdType.MESH
        )
    pl.semaphore_wait(barrier, len(partners))


def sending(source, target, send_sem, recv_sem, partner):
    return pltpu.make_async_remote_copy(
        src_ref=source,
        dst_ref=target,
        send_sem=send_sem,
        recv_sem=recv_sem,
        device_id=partner,
        device_id_type=pl.DeviceIdType.MESH,
    )


def scan_kernel(
    clique,
    outer,
    state_ref,
    decay_ref,
    weight_ref,
    out_ref,
    onward_ref,
    near,
    near_decay,
    prefix,
    before,
    whole,
    whole_decay,
    far,
    far_decay,
    carry,
    replies,
    near_sems,
    far_sems,
    reply_sems,
    ring_sems,
):
    me = lax.axis_index("sp")
    spot = lax.rem(me, clique)
    layer = me // clique
    base = me - spot
    mates = [lax.rem(spot + d, clique) for d in range(1, clique)]
    layers = [lax.rem(layer + d, outer) for d in range(1, outer)]
    greet(
        [{"sp": base + mate} for mate in mates]
        + [{"sp": other * clique + spot} for other in layers]
    )

    ring = sending(
        weight_ref,
        onward_ref,
        ring_sems.at[0],
        ring_sems.at[1],
        {"sp": lax.rem(layer + 1, outer) * clique + spot},
    )
    if outer > 1:
        ring.start()

    def near_copy(mate, slot, sem_slot):
        who = {"sp": base + mate}
        return (
            sending(
                state_ref.at[mate],
                near.at[slot],
                near_sems.at[0, mate],
                near_sems.at[1, sem_slot],
                who,
            ),
            sending(
                decay_ref.at[mate],
                near_decay.at[slot],
                near_sems.at[2, mate],
                near_sems.at[3, sem_slot],
                who,
            ),
        )

    for mate in mates:
        for copy in near_copy(mate, spot, spot):
            copy.start()
    near[spot] = state_ref[spot]
    near_decay[spot] = decay_ref[spot]
    for mate in mates:
        for copy in near_copy(mate, mate, mate):
            copy.wait_recv()
    for way in range(2):
        order = range(clique) if way == 0 else range(clique - 1, -1, -1)
        running = jnp.zeros(prefix.shape[2:], jnp.float32)
        product = jnp.ones(before.shape[2:], jnp.float32)
        for turn in order:
            prefix[turn, way] = running
            before[turn, way] = product
            factor = near_decay[turn, way]
            running = running * factor[:, None, :] + near[turn, way].astype(jnp.float32)
            product = product * factor
        whole[way] = running.astype(jnp.bfloat16)
        whole_decay[way] = product

    def far_copy(way, other, slot):
        who = {"sp": other * clique + spot}
        return (
            sending(
                whole.at[way],
                far.at[way, slot],
                far_sems.at[0, way, other],
                far_sems.at[1, way, slot],
                who,
            ),
            sending(
                whole_decay.at[way],
                far_decay.at[way, slot],
                far_sems.at[2, way, other],
                far_sems.at[3, way, slot],
                who,
            ),
        )

    def later(way, first, second):
        return second > first if way == 0 else second < first

    for other in layers:
        for way in range(2):

            @pl.when(later(way, layer, other))
            def _():
                for copy in far_copy(way, other, layer):
                    copy.start()

    carry[...] = jnp.zeros_like(carry)
    for way in range(2):
        order = range(outer) if way == 0 else range(outer - 1, -1, -1)
        for other in order:

            @pl.when(later(way, other, layer))
            def _():
                for copy in far_copy(way, other, other):
                    copy.wait_recv()
                carry[way] = carry[way] * far_decay[way, other][:, None, :] + far[
                    way, other
                ].astype(jnp.float32)

    for turn in range(clique):
        for way in range(2):
            replies[turn, way] = (
                prefix[turn, way] + carry[way] * before[turn, way][:, None, :]
            ).astype(jnp.bfloat16)

    def reply(mate, slot):
        return sending(
            replies.at[mate],
            out_ref.at[slot],
            reply_sems.at[0, mate],
            reply_sems.at[1, slot],
            {"sp": base + mate},
        )

    for mate in mates:
        reply(mate, spot).start()
    out_ref[spot] = replies[spot]
    for mate in mates:
        reply(mate, mate).wait_recv()
    for mate in mates:
        for copy in near_copy(mate, spot, spot):
            copy.wait_send()
        reply(mate, spot).wait_send()
    for other in layers:
        for way in range(2):

            @pl.when(later(way, layer, other))
            def _():
                for copy in far_copy(way, other, layer):
                    copy.wait_send()

    if outer > 1:
        ring.wait()


def scan_states(states, decays, weight):
    count = lax.axis_size("sp")
    clique = clique_of(count)
    outer = count // clique
    ways, heads, rows, cols = states.shape
    part = heads // clique
    states = states.reshape(ways, clique, part, rows, cols).transpose(1, 0, 2, 3, 4)
    decays = jnp.broadcast_to(
        decays.reshape(ways, clique, part).transpose(1, 0, 2)[..., None],
        (clique, ways, part, cols),
    )
    block = (part, rows, cols)
    whole_out, onward = pl.pallas_call(
        functools.partial(scan_kernel, clique, outer),
        out_shape=(
            jax.ShapeDtypeStruct((clique, ways) + block, jnp.bfloat16),
            jax.ShapeDtypeStruct(weight.shape, weight.dtype),
        ),
        in_specs=[pl.BlockSpec(memory_space=pltpu.VMEM)] * 2
        + [pl.BlockSpec(memory_space=pl.ANY)],
        out_specs=(
            pl.BlockSpec(memory_space=pltpu.VMEM),
            pl.BlockSpec(memory_space=pl.ANY),
        ),
        scratch_shapes=[
            pltpu.VMEM((clique, ways) + block, jnp.bfloat16),
            pltpu.VMEM((clique, ways, part, cols), jnp.float32),
            pltpu.VMEM((clique, ways) + block, jnp.float32),
            pltpu.VMEM((clique, ways, part, cols), jnp.float32),
            pltpu.VMEM((ways,) + block, jnp.bfloat16),
            pltpu.VMEM((ways, part, cols), jnp.float32),
            pltpu.VMEM((ways, outer) + block, jnp.bfloat16),
            pltpu.VMEM((ways, outer, part, cols), jnp.float32),
            pltpu.VMEM((ways,) + block, jnp.float32),
            pltpu.VMEM((clique, ways) + block, jnp.bfloat16),
            pltpu.SemaphoreType.DMA((4, clique)),
            pltpu.SemaphoreType.DMA((4, 2, outer)),
            pltpu.SemaphoreType.DMA((2, clique)),
            pltpu.SemaphoreType.DMA((2,)),
        ],
        compiler_params=pltpu.CompilerParams(collective_id=1, has_side_effects=True),
        cost_estimate=pl.CostEstimate(
            flops=0, bytes_accessed=320 * states.size, transcendentals=0
        ),
    )(states.astype(jnp.bfloat16), decays, weight)
    return whole_out.transpose(1, 0, 2, 3, 4).reshape(ways, heads, rows, cols), onward


def project_kernel(clique, outer, tps, mixed_ref, *rest):
    given = max(outer - 1, 1)
    weight_refs = list(rest[:given])
    (
        out_ref,
        gathered,
        partial,
        pieces,
        summed,
        mixed_sems,
        piece_sems,
        out_sems,
        last,
        ring_sems,
    ) = rest[given:]
    me = lax.axis_index("sp")
    lane = lax.axis_index("tp")
    spot = lax.rem(me, clique)
    layer = me // clique
    base = me - spot
    flips = list(range(1, clique))
    lanes = [lax.rem(lane + d, tps) for d in range(1, tps)]

    def at_flip(flip):
        return {"sp": base + flipped(spot, flip)}

    after = {"sp": lax.rem(layer + 1, outer) * clique + spot}
    prior = {"sp": lax.rem(layer + outer - 1, outer) * clique + spot}
    greet(
        [at_flip(flip) for flip in flips]
        + [{"tp": other} for other in lanes]
        + ([after, prior] if outer > 1 else [])
    )
    ring = sending(weight_refs[-1], last, ring_sems.at[0], ring_sems.at[1], after)
    if outer > 1:
        ring.start()
        weight_refs = weight_refs + [last]
    share = mixed_ref.shape[1] // tps

    def mixed_copy(flip):
        low = flip & -flip
        high = flip - low
        return sending(
            gathered.at[high] if high else mixed_ref,
            gathered.at[flip],
            mixed_sems.at[0, flip],
            mixed_sems.at[1, flip],
            at_flip(low),
        )

    def piece_copy(flip, other, slot):
        return sending(
            partial.at[flip, other],
            pieces.at[flip, slot],
            piece_sems.at[0, flip, other],
            piece_sems.at[1, flip, slot],
            {"tp": other},
        )

    def out_copy(flip, slot):
        return sending(
            summed.at[flip],
            out_ref.at[slot],
            out_sems.at[0, flip],
            out_sems.at[1, flip],
            at_flip(flip),
        )

    for flip in reversed(flips):
        if flip & (flip - 1) == 0:
            mixed_copy(flip).start()

    def multiply(flip, turns):
        source = gathered.at[flip] if flip else mixed_ref
        for turn in turns:
            weight_ref = weight_refs[turn]
            column = lax.rem(layer + outer - turn, outer)
            product = jnp.dot(
                source[0], weight_ref[0], preferred_element_type=jnp.float32
            ) + jnp.dot(source[1], weight_ref[1], preferred_element_type=jnp.float32)
            rounded = product.astype(jnp.bfloat16)
            for other in range(tps):
                partial[flip, other, column] = rounded[other * share : (other + 1) * share]

    def settle(flip):
        total = partial[flip, lane].astype(jnp.float32)
        for other in lanes:
            piece_copy(flip, other, other).wait_recv()
            total = total + pieces[flip, other].astype(jnp.float32)
        if flip:
            summed[flip] = total.astype(jnp.bfloat16)
            out_copy(flip, spot).start()
        else:
            out_ref[spot] = total.astype(jnp.bfloat16)

    for flip in range(clique):
        if flip:
            mixed_copy(flip).wait_recv()
            for further in flips:
                if further != flip and further - (further & -further) == flip:
                    mixed_copy(further).start()
        multiply(flip, range(given))
    if outer > 1:
        ring.wait_recv()
    for flip in range(clique):
        multiply(flip, range(given, outer))
        for other in lanes:
            piece_copy(flip, other, lane).start()
        if flip:
            settle(flip - 1)
    settle(clique - 1)
    for flip in flips:
        out_copy(flip, flipped(spot, flip)).wait_recv()
    for flip in flips:
        mixed_copy(flip).wait_send()
        out_copy(flip, spot).wait_send()
    for flip in range(clique):
        for other in lanes:
            piece_copy(flip, other, lane).wait_send()
    if outer > 1:
        ring.wait_send()


def ring_weights(held, limit):
    count = lax.axis_size("sp")
    clique = clique_of(count)
    outer = count // clique
    pairs = [(i, (i + clique) % count) for i in range(count)]
    goal = max(outer + limit, 1) if limit < 0 else min(limit, outer)
    held = held[: max(outer - 1, 1)]
    while len(held) < goal:
        held = held + [lax.ppermute(held[-1], "sp", pairs)]
    return held


def flipped(spot, flip):
    bit = 1
    while bit <= flip:
        if flip & bit:
            spot = spot + bit - 2 * bit * lax.rem(spot // bit, 2)
        bit *= 2
    return spot


def project(mixed, weights):
    count = lax.axis_size("sp")
    tps = lax.axis_size("tp")
    clique = clique_of(count)
    outer = count // clique
    rows = mixed.shape[1]
    width = weights[0].shape[2]
    share = rows // tps
    block = (outer, share, width)
    out = pl.pallas_call(
        functools.partial(project_kernel, clique, outer, tps),
        out_shape=jax.ShapeDtypeStruct((clique,) + block, jnp.bfloat16),
        in_specs=[pl.BlockSpec(memory_space=pltpu.VMEM)] * (1 + len(weights)),
        out_specs=pl.BlockSpec(memory_space=pltpu.VMEM),
        scratch_shapes=[
            pltpu.VMEM((clique,) + mixed.shape, jnp.bfloat16),
            pltpu.VMEM((clique, tps) + block, jnp.bfloat16),
            pltpu.VMEM((clique, tps) + block, jnp.bfloat16),
            pltpu.VMEM((clique,) + block, jnp.bfloat16),
            pltpu.SemaphoreType.DMA((2, clique)),
            pltpu.SemaphoreType.DMA((2, clique, tps)),
            pltpu.SemaphoreType.DMA((2, clique)),
            pltpu.VMEM(weights[0].shape, weights[0].dtype),
            pltpu.SemaphoreType.DMA((2,)),
        ],
        compiler_params=pltpu.CompilerParams(collective_id=2, has_side_effects=True),
    )(mixed, *weights)
    return out.transpose(2, 1, 0, 3).reshape(share, outer * clique * width)


def rotate(matrix, offset):
    row_count = matrix.shape[0]
    halfway = HEAD // 2
    heads_here = matrix.shape[1] // HEAD
    spacing = ROTARY_BASE ** (-jnp.arange(halfway, dtype=jnp.float32) * 2.0 / HEAD)
    places = (offset + jnp.arange(row_count, dtype=jnp.int32)).astype(jnp.float32)
    angles = places[:, None] * spacing[None, :]
    cosine = jnp.cos(angles)[:, None, :]
    sine_table = jnp.sin(angles)[:, None, :]
    halves = matrix.astype(jnp.float32).reshape(row_count, heads_here, 2, halfway)
    former = halves[:, :, 0]
    latter = halves[:, :, 1]
    turned = jnp.stack(
        [former * cosine - latter * sine_table, latter * cosine + former * sine_table], axis=2
    )
    return turned.reshape(row_count, heads_here * HEAD).astype(jnp.bfloat16)


def banded(matrix, block_count, kv_here):
    stacked = matrix.reshape(block_count + 2, SPAN, kv_here, HEAD)
    return jnp.concatenate([stacked[:-2], stacked[1:-1], stacked[2:]], axis=1)


def attend(turned_queries, key_band, value_band, absorber_score_vector, offset, seq_total):
    row_count = turned_queries.shape[0]
    block_count = row_count // SPAN
    kv_here = key_band.shape[1] // HEAD
    sharing = turned_queries.shape[1] // HEAD // kv_here
    key_tiles = banded(key_band, block_count, kv_here)
    value_tiles = banded(value_band, block_count, kv_here)
    query_tiles = turned_queries.reshape(block_count, SPAN, kv_here, sharing, HEAD)
    scores = jnp.einsum(
        "bqkgd,bskd->bkgqs", query_tiles, key_tiles, preferred_element_type=jnp.float32
    ) * HEAD ** (-0.5)
    within = jnp.arange(SPAN, dtype=jnp.int32)[:, None]
    across = jnp.arange(3 * SPAN, dtype=jnp.int32)[None, :]
    inside = jnp.abs(across - SPAN - within) <= WINDOW
    places = offset - SPAN + jnp.arange(block_count, dtype=jnp.int32)[:, None] * SPAN + across
    present = (places >= 0) & (places < seq_total)
    allowed = inside[None, :, :] & present[:, None, :]
    scores = jnp.where(allowed[:, None, None, :, :], scores, -jnp.inf)
    sink_rows = absorber_score_vector.reshape(kv_here, sharing)[None, :, :, None, None]
    ceiling = jnp.maximum(jnp.max(scores, axis=-1, keepdims=True), sink_rows)
    weights = jnp.exp(scores - ceiling)
    denominator = jnp.sum(weights, axis=-1, keepdims=True) + jnp.exp(sink_rows - ceiling)
    probabilities = (weights / denominator).astype(jnp.bfloat16)
    attended = jnp.einsum(
        "bkgqs,bskd->bqkgd", probabilities, value_tiles, preferred_element_type=jnp.float32
    )
    return attended.reshape(row_count, turned_queries.shape[1]).astype(jnp.bfloat16)


def convolve(padded, taps_all, row_count):
    summed = jnp.zeros((row_count, padded.shape[1]), jnp.float32)
    for tap_index in range(CONV):
        summed = summed + padded[tap_index : tap_index + row_count].astype(jnp.float32) * taps_all[
            tap_index
        ].astype(jnp.float32)
    return jax.nn.silu(summed).astype(jnp.bfloat16)


def prepare(scan_rows, step_rows, decay_rows, write_rows, read_rows):
    row_count = scan_rows.shape[0]
    block_count = row_count // SPAN
    groups_here = write_rows.shape[1]
    per_group = scan_rows.shape[2]
    step_tiles = step_rows.reshape(block_count, SPAN, groups_here, per_group)
    scaled = (
        scan_rows.astype(jnp.float32).reshape(block_count, SPAN, groups_here, per_group, SSD_HEAD)
        * step_tiles[..., None]
    )
    running = jnp.cumsum(decay_rows.reshape(block_count, SPAN, groups_here, per_group), axis=1)
    write_tiles = write_rows.reshape(block_count, SPAN, groups_here, STATE)
    read_tiles = read_rows.reshape(block_count, SPAN, groups_here, STATE)
    earlier_mask = jnp.arange(SPAN)[:, None] >= jnp.arange(SPAN)[None, :]
    spread = running[:, :, None] - running[:, None, :]
    fading = jnp.exp(jnp.where(earlier_mask[None, :, :, None, None], spread, -jnp.inf))
    affinity = jnp.einsum(
        "blgn,bsgn->blsg", read_tiles, write_tiles, preferred_element_type=jnp.float32
    )
    within_block = jnp.einsum(
        "blsgr,bsgrp->blgrp", affinity[..., None] * fading, scaled
    )
    to_end = jnp.exp(running[:, -1:] - running)
    block_states = jnp.einsum(
        "blgn,blgrp->bgrpn",
        write_tiles.astype(jnp.float32),
        scaled * to_end[..., None],
    )
    totals = running[:, -1]

    def advance(carried, block_item):
        fresh_state, block_total = block_item
        return (carried * jnp.exp(block_total)[..., None, None] + fresh_state, carried)

    final_state, entering = lax.scan(
        advance, jnp.zeros(block_states.shape[1:], jnp.float32), (block_states, totals)
    )
    summary = (jnp.exp(jnp.sum(totals, axis=0)), final_state)
    return ((within_block, entering, running, totals, read_tiles), summary)


def finish(pieces, incoming):
    within_block, entering, running, totals, read_tiles = pieces
    before = jnp.cumsum(totals, axis=0) - totals
    starting = entering + incoming[None] * jnp.exp(before)[..., None, None]
    carried = (
        jnp.einsum(
            "blgn,bgrpn->blgrp",
            read_tiles.astype(jnp.float32),
            starting,
        )
        * jnp.exp(running)[..., None]
    )
    joined = within_block + carried
    return joined.reshape(joined.shape[0] * SPAN, -1)


def local(
    asking_matrix,
    matching_key_matrix,
    carried_value_matrix,
    silu_switch_argument,
    duality_source_matrix,
    storing_direction_matrix,
    fetching_direction_matrix,
    duality_kernel_coefficients,
    storing_kernel_coefficients,
    fetching_kernel_coefficients,
    raw_increment_lengths,
    logarithmic_fading_speeds,
    token_fading_spikes,
    absorber_score_vector,
    cluster_scaling_factor,
    final_mapping_matrix,
):
    row_count = asking_matrix.shape[0]
    offset = lax.axis_index("sp") * row_count
    seq_total = lax.axis_size("sp") * row_count
    weights = ring_weights([final_mapping_matrix], 2)
    turned_queries = rotate(asking_matrix, offset)
    key_value = jnp.concatenate([rotate(matching_key_matrix, offset), carried_value_matrix], axis=1)
    raw_rows = jnp.concatenate(
        [duality_source_matrix, storing_direction_matrix, fetching_direction_matrix], axis=1
    )
    margin = CONV // 2
    pair_rims = padded_2(key_value, (("sp", 0),), WINDOW)
    raw_rims = padded_2(raw_rows, (("sp", 0),), margin)
    filler = jnp.zeros((SPAN - WINDOW, key_value.shape[1]), jnp.bfloat16)
    pair_band = jnp.concatenate([filler, pair_rims, filler], axis=0)
    kv_width = matching_key_matrix.shape[1]
    conved = convolve(
        raw_rims,
        jnp.concatenate(
            [
                duality_kernel_coefficients,
                storing_kernel_coefficients,
                fetching_kernel_coefficients,
            ],
            axis=1,
        ),
        row_count,
    )
    scan_width = duality_source_matrix.shape[1]
    write_width = storing_direction_matrix.shape[1]
    groups_here = write_width // STATE
    per_group = scan_width // SSD_HEAD // groups_here
    scan_rows = conved[:, :scan_width].reshape(row_count, groups_here, per_group, SSD_HEAD)
    write_rows = conved[:, scan_width : scan_width + write_width].reshape(
        row_count, groups_here, STATE
    )
    read_rows = conved[:, scan_width + write_width :].reshape(row_count, groups_here, STATE)
    joint_increment_lengths = jax.nn.softplus(raw_increment_lengths)
    joint_fading_amounts = (
        -jnp.exp(logarithmic_fading_speeds)[:, :, None] * joint_increment_lengths
        + token_fading_spikes
    )
    steps_rows = jnp.transpose(joint_increment_lengths, (0, 2, 1)).reshape(
        2, row_count, groups_here, per_group
    )
    decay_rows = jnp.transpose(joint_fading_amounts, (0, 2, 1)).reshape(
        2, row_count, groups_here, per_group
    )
    ahead_pieces, ahead_summary = prepare(
        scan_rows, steps_rows[0], decay_rows[0], write_rows, read_rows
    )
    back_pieces, back_summary = prepare(
        scan_rows[::-1], steps_rows[1][::-1], decay_rows[1][::-1], write_rows[::-1], read_rows[::-1]
    )
    heads = groups_here * per_group
    incoming, onward = scan_states(
        jnp.stack([ahead_summary[1], back_summary[1]]).reshape(2, heads, SSD_HEAD, STATE),
        jnp.stack([ahead_summary[0], back_summary[0]]).reshape(2, heads),
        weights[-1],
    )
    weights = ring_weights(weights + [onward], -1)
    incoming = incoming.reshape(2, groups_here, per_group, SSD_HEAD, STATE)
    turned_queries, incoming = lax.optimization_barrier((turned_queries, incoming))
    attended = attend(
        turned_queries,
        pair_band[:, :kv_width],
        pair_band[:, kv_width:],
        absorber_score_vector,
        offset,
        seq_total,
    )
    both_ways = finish(ahead_pieces, incoming[0].astype(jnp.float32)) + finish(
        back_pieces, incoming[1].astype(jnp.float32)
    )[::-1]
    gated_rows = both_ways * jax.nn.silu(silu_switch_argument.astype(jnp.float32))
    grouped = gated_rows.reshape(row_count, groups_here, -1)
    grouped = grouped * lax.rsqrt(jnp.mean(grouped * grouped, axis=-1, keepdims=True) + EPSILON)
    normed = (grouped.reshape(row_count, scan_width) * cluster_scaling_factor).astype(jnp.bfloat16)
    return project(jnp.stack([attended, normed]), weights)


def solution(mesh):
    in_specs = (
        P("sp", "tp"),
        P("sp", "tp"),
        P("sp", "tp"),
        P("sp", "tp"),
        P("sp", "tp"),
        P("sp", "tp"),
        P("sp", "tp"),
        P(None, "tp"),
        P(None, "tp"),
        P(None, "tp"),
        P(None, "tp", "sp"),
        P(None, "tp"),
        P(None, "tp", "sp"),
        P("tp"),
        P("tp"),
        P(None, "tp", "sp"),
    )
    out_specs = P(("sp", "tp"), None)
    return jax.shard_map(local, mesh=mesh, in_specs=in_specs, out_specs=out_specs, check_vma=False)
```

profile of v0, /device:TPU:0, one launch (start us, length us, event | category | flops | bytes accessed | tf_op | source)
XLA Modules:
  0.0 147.9 jit_solution(12837175990119012125)
XLA Ops:
  0.0 1.1 copy.118
  1.1 1.0 copy.117
  2.2 0.2 multiply_cosine_fusion
  2.4 0.7 pad_maximum_fusion.3
  3.2 1.3 collective-permute-start.1
  4.5 3.8 %collective-permute-start = (bf16[128,1024]{0,1:T(8,128)(2,1)}, bf16[128,1024]{0,1:T(8,128)(2,1)}, u32[]{:S(2)}, u32[]{:S(2)}) collective-permute-start(bf16[128,1024]{0,1:T(8,128)(2,1)} %pad_maximum_fusion.3), channel_id=1, source_target_pairs={{0,2},{2,4},{4,6},{6,8},{8,10},{10,12},{12,14},{14,16},{16,18},{18... | collective-permute-start | bytes 786440 | tf_op jit(solution)/shard_map/ppermute | solution.py:30
  8.7 1.1 fusion.74
  9.9 4.8 %collective-permute-start.2 = (bf16[2,2048]{0,1:T(8,128)(2,1)}, bf16[2,2048]{0,1:T(8,128)(2,1)}, u32[]{:S(2)}, u32[]{:S(2)}) collective-permute-start(bf16[2,2048]{0,1:T(8,128)(2,1)} %get-tuple-element.49), channel_id=1, source_target_pairs={{0,2},{2,4},{4,6},{6,8},{8,10},{10,12},{12,14},{14,16},{16,18},{18... | collective-permute-start | bytes 24584 | tf_op jit(solution)/shard_map/ppermute | solution.py:30
  14.7 1.3 collective-permute-start.3
  16.0 3.3 %collective-permute-start.4 = (bf16[2,1024,256]{2,1,0:T(8,128)(2,1)}, bf16[2,1024,256]{2,1,0:T(8,128)(2,1)S(1)}, u32[]{:S(2)}, u32[]{:S(2)}) collective-permute-start(bf16[2,1024,256]{2,1,0:T(8,128)(2,1)} %rest_0_.1), channel_id=1, source_target_pairs={{0,8},{2,10},{4,12},{6,14},{8,16},{10,18},{12,20},{14,22},{16,24},... | collective-permute-start | bytes 3145736 | tf_op jit(solution)/shard_map/ppermute | solution.py:405
  19.4 0.6 fusion.77
  20.3 0.6 exponential_bitcast_fusion.1
  20.9 0.6 exponential_multiply_fusion.1
  21.8 0.6 exponential_bitcast_fusion
  22.4 0.6 subtract_exponential_fusion.3
  23.0 0.6 iota_compare_fusion
  23.6 0.6 iota_add_fusion.1
  24.2 0.6 slice_convert_fusion.4
  25.2 0.7 subtract_convert_fusion
  26.1 1.6 %pad_maximum_fusion.4 = bf16[128,8,2,64]{0,3,2,1:T(8,128)(2,1)} fusion(bf16[128,8,1,64]{0,3,2,1:T(8,128)(2,1)} %get-tuple-element.44, bf16[128,8,1,64]{0,3,2,1:T(8,128)(2,1)S(1)} %get-tuple-element.42), kind=kLoop, calls=%fused_computation.76 | loop fusion | flops 131072 | bytes 524288 | tf_op jit(solution)/shard_map/stack | solution.py:460
  27.8 0.8 fusion.61
  28.6 0.7 maximum_bitcast_fusion.5
  29.7 0.6 copy.133
  30.3 0.7 copy.140
  31.1 0.7 copy.147
  32.0 1.3 max.28
  33.4 1.8 %maximum_maximum_fusion = (bf16[130,2048]{0,1:T(8,128)(2,1)S(1)}, bf16[130,2048]{0,1:T(8,128)(2,1)S(1)}) fusion(bf16[128,512]{0,1:T(8,128)(2,1)S(1)} %copy.127, bf16[128,512]{0,1:T(8,128)(2,1)S(1)} %copy.126, bf16[128,1024]{0,1:T(8,128)(2,1)S(1)} %copy.125, bf16[2,2048]{0,1:T(8,128)(2,1)} %collective-permute-done.2, bf16[2,2048]{0,1:T(8,128)(2,1)} %collective-permute-done.3), kind=kLoop, calls=%fused_computation.21 | loop fusion | flops 4259840 | bytes 1605632 | tf_op jit(solution)/shard_map/concatenate | solution.py:28
  35.3 4.5 %multiply_convert_fusion = bf16[128,2048]{0,1:T(8,128)(2,1)S(1)} fusion(bf16[130,2048]{0,1:T(8,128)(2,1)S(1)} %get-tuple-element.48, bf16[130,2048]{0,1:T(8,128)(2,1)S(1)} %get-tuple-element.47, f32[2048]{0:T(1024)S(1)} %bitcast.194, f32[2048]{0:T(1024)S(1)} %bitcast.195, f32[2048]{0:T(1024)S(1)} %bitcast.196, f32[2048]{0:T(1024)S(1)} %bitcast.197, ...), kind=kLoop, calls=%fused_computation.31 | loop fusion | flops 6291456 | bytes 3186688 | tf_op jit(solution)/shard_map/convert_element_type | solution.py:506
  39.8 0.4 rev.21
  40.3 0.2 convolution_bitcast_fusion.5
  40.5 0.4 rev.22
  40.9 0.2 rev.19
  41.1 0.2 fusion.7
  41.3 0.2 convolution_bitcast_fusion.4
  41.6 0.2 fusion.8
  41.9 0.8 maximum_bitcast_fusion.state_ref
  43.0 1.6 %fusion.76 = (bf16[128,512]{0,1:T(8,128)(2,1)}, bf16[128,512]{0,1:T(8,128)(2,1)S(1)}) fusion(bf16[128,1024]{0,1:T(8,128)(2,1)} %collective-permute-done.1), kind=kLoop, calls=%fused_computation.143 | loop fusion | bytes 524288 | tf_op jit(solution)/shard_map/slice | solution.py:468
  44.8 1.6 %fusion.75 = (bf16[128,512]{0,1:T(8,128)(2,1)}, bf16[128,512]{0,1:T(8,128)(2,1)S(1)}) fusion(bf16[128,1024]{0,1:T(8,128)(2,1)} %collective-permute-done), kind=kLoop, calls=%fused_computation.142 | loop fusion | bytes 524288 | tf_op jit(solution)/shard_map/slice | solution.py:468
  46.4 0.8 copy.120
  47.2 2.7 %collective-permute-done.4.weight_ref.rest_1_ = bf16[2,1024,256]{2,1,0:T(8,128)(2,1)S(1)} collective-permute-done((bf16[2,1024,256]{2,1,0:T(8,128)(2,1)}, bf16[2,1024,256]{2,1,0:T(8,128)(2,1)S(1)}, u32[]{:S(2)}, u32[]{:S(2)}) %collective-permute-start.4) | collective-permute-done | bytes 1048608 | tf_op jit(solution)/shard_map/ppermute | solution.py:405
  49.8 0.8 broadcast_in_dim.37.decay_ref
  50.6 0.2 copy-done
  50.9 37.2 %shard_map.154 = (bf16[4,2,4,64,128]{4,3,2,1,0:T(8,128)(2,1)}, bf16[2,1024,256]{2,1,0:T(8,128)(2,1)}) custom-call(bf16[4,2,4,64,128]{4,3,2,1,0:T(8,128)(2,1)} %maximum_bitcast_fusion.state_ref, f32[4,2,4,128]{3,2,1,0:T(4,128)} %broadcast_in_dim.37.decay_ref, bf16[2,1024,256]{2,1,0:T(8,128)(2,1)} %copy-done), custom_call_target="tpu_custom_call" | custom-call | bytes 83886080 | tf_op jit(solution)/shard_map/pallas_call | solution.py:238
  88.0 1.2 fusion.3
  89.3 0.5 fusion.2
  89.9 0.2 copy.152
  90.1 0.2 copy-done.2
  90.3 0.3 fusion.4
  90.7 0.6 fusion.1
  91.2 0.2 copy.151
  91.4 0.2 rev.23
  91.7 0.2 fusion.72
  91.9 0.2 mul.423
  92.2 0.2 reduce_sum.20
  92.4 0.2 mul.424
  92.9 0.4 fusion.79
  93.2 0.2 copy-done.17
  93.5 0.2 fusion
  93.9 0.4 convolution_convert_fusion
  94.5 0.2 fusion.48
  94.8 0.8 pad_maximum_fusion.2.mixed_ref
  95.6 49.7 %shard_map.155 = bf16[4,4,64,256]{3,2,1,0:T(8,128)(2,1)} custom-call(bf16[2,128,1024]{2,1,0:T(8,128)(2,1)} %pad_maximum_fusion.2.mixed_ref, bf16[2,1024,256]{2,1,0:T(8,128)(2,1)} %rest_0_.1, bf16[2,1024,256]{2,1,0:T(8,128)(2,1)} %copy-done, bf16[2,1024,256]{2,1,0:T(8,128)(2,1)} %get-tuple-element.40.rest_2_), custom_call_target="tpu_custom_call" | custom-call | tf_op jit(solution)/shard_map/pallas_call | solution.py:427
  145.3 1.4 copy.155
  146.7 1.2 reshape.504
  (117 shorter events, 3.7 us)
Async XLA Ops:
  0.0 8.2 %copy-start.6 = (bf16[128,512]{1,0:T(8,128)(2,1)S(1)}, bf16[128,512]{1,0:T(8,128)(2,1)}, u32[]{:S(2)}) copy-start(bf16[128,512]{1,0:T(8,128)(2,1)} %param.22) | copy-start | bytes 393220
  0.0 8.3 %copy-start.7 = (bf16[128,512]{1,0:T(8,128)(2,1)S(1)}, bf16[128,512]{1,0:T(8,128)(2,1)}, u32[]{:S(2)}) copy-start(bf16[128,512]{1,0:T(8,128)(2,1)} %param.21) | copy-start | bytes 393220
  0.0 8.5 %copy-start.3 = (bf16[128,1024]{1,0:T(8,128)(2,1)S(1)}, bf16[128,1024]{1,0:T(8,128)(2,1)}, u32[]{:S(2)}) copy-start(bf16[128,1024]{1,0:T(8,128)(2,1)} %param.20) | copy-start | bytes 786436
  3.2 39.8 %collective-permute-start.1 = (bf16[128,1024]{0,1:T(8,128)(2,1)}, bf16[128,1024]{0,1:T(8,128)(2,1)}, u32[]{:S(2)}, u32[]{:S(2)}) collective-permute-start(bf16[128,1024]{0,1:T(8,128)(2,1)} %pad_maximum_fusion.3), channel_id=1, source_target_pairs={{2,0},{4,2},{6,4},{8,6},{10,8},{12,10},{14,12},{16,14},{18,16},{20... | collective-permute-start | bytes 786440 | tf_op jit(solution)/shard_map/ppermute | solution.py:32
  4.5 40.3 %collective-permute-start = (bf16[128,1024]{0,1:T(8,128)(2,1)}, bf16[128,1024]{0,1:T(8,128)(2,1)}, u32[]{:S(2)}, u32[]{:S(2)}) collective-permute-start(bf16[128,1024]{0,1:T(8,128)(2,1)} %pad_maximum_fusion.3), channel_id=1, source_target_pairs={{0,2},{2,4},{4,6},{6,8},{8,10},{10,12},{12,14},{14,16},{16,18},{18... | collective-permute-start | bytes 786440 | tf_op jit(solution)/shard_map/ppermute | solution.py:30
  8.7 10.6 %copy-start.37 = (f32[2,16]{1,0:T(2,128)S(1)}, f32[2,16]{1,0:T(2,128)}, u32[]{:S(2)}) copy-start(f32[2,16]{1,0:T(2,128)} %param.27) | copy-start | bytes 388
  8.7 10.6 %copy-start.21 = (f32[2,16,128]{2,1,0:T(8,128)S(1)}, f32[2,16,128]{2,1,0:T(8,128)}, u32[]{:S(2)}) copy-start(f32[2,16,128]{2,1,0:T(8,128)} %param.26) | copy-start | bytes 49156
  8.7 10.6 %copy-start.22 = (f32[2,16,128]{2,1,0:T(8,128)S(1)}, f32[2,16,128]{2,1,0:T(8,128)}, u32[]{:S(2)}) copy-start(f32[2,16,128]{2,1,0:T(8,128)} %param.28) | copy-start | bytes 49156
  9.9 14.3 %copy-start.19 = (bf16[5,1024]{1,0:T(8,128)(2,1)S(1)}, bf16[5,1024]{1,0:T(8,128)(2,1)}, u32[]{:S(2)}) copy-start(bf16[5,1024]{1,0:T(8,128)(2,1)} %param.23) | copy-start | bytes 30724
  9.9 14.3 %copy-start.28 = (bf16[5,512]{1,0:T(8,128)(2,1)S(1)}, bf16[5,512]{1,0:T(8,128)(2,1)}, u32[]{:S(2)}) copy-start(bf16[5,512]{1,0:T(8,128)(2,1)} %param.24) | copy-start | bytes 15364
  9.9 14.3 %copy-start.29 = (bf16[5,512]{1,0:T(8,128)(2,1)S(1)}, bf16[5,512]{1,0:T(8,128)(2,1)}, u32[]{:S(2)}) copy-start(bf16[5,512]{1,0:T(8,128)(2,1)} %param.25) | copy-start | bytes 15364
  9.9 23.5 %collective-permute-start.2 = (bf16[2,2048]{0,1:T(8,128)(2,1)}, bf16[2,2048]{0,1:T(8,128)(2,1)}, u32[]{:S(2)}, u32[]{:S(2)}) collective-permute-start(bf16[2,2048]{0,1:T(8,128)(2,1)} %get-tuple-element.49), channel_id=1, source_target_pairs={{0,2},{2,4},{4,6},{6,8},{8,10},{10,12},{12,14},{14,16},{16,18},{18... | collective-permute-start | bytes 24584 | tf_op jit(solution)/shard_map/ppermute | solution.py:30
  14.7 18.7 %collective-permute-start.3 = (bf16[2,2048]{0,1:T(8,128)(2,1)}, bf16[2,2048]{0,1:T(8,128)(2,1)}, u32[]{:S(2)}, u32[]{:S(2)}) collective-permute-start(bf16[2,2048]{0,1:T(8,128)(2,1)} %get-tuple-element.50), channel_id=1, source_target_pairs={{2,0},{4,2},{6,4},{8,6},{10,8},{12,10},{14,12},{16,14},{18,16},{20... | collective-permute-start | bytes 24584 | tf_op jit(solution)/shard_map/ppermute | solution.py:32
  16.0 33.9 %collective-permute-start.4 = (bf16[2,1024,256]{2,1,0:T(8,128)(2,1)}, bf16[2,1024,256]{2,1,0:T(8,128)(2,1)S(1)}, u32[]{:S(2)}, u32[]{:S(2)}) collective-permute-start(bf16[2,1024,256]{2,1,0:T(8,128)(2,1)} %rest_0_.1), channel_id=1, source_target_pairs={{0,8},{2,10},{4,12},{6,14},{8,16},{10,18},{12,20},{14,22},{16,24},... | collective-permute-start | bytes 3145736 | tf_op jit(solution)/shard_map/ppermute | solution.py:405
  19.4 5.6 %copy-start.4 = (bf16[128,1024]{1,0:T(8,128)(2,1)S(1)}, bf16[128,1024]{1,0:T(8,128)(2,1)}, u32[]{:S(2)}) copy-start(bf16[128,1024]{1,0:T(8,128)(2,1)} %param.16) | copy-start | bytes 786436
  25.2 2.6 %copy-start.27 = (s32[384]{0:T(512)S(1)}, s32[384]{0:T(512)}, u32[]{:S(2)}) copy-start(s32[384]{0:T(512)} %iota_add_fusion.1) | copy-start | bytes 4612
  29.6 11.5 %copy-start.30 = (f32[128,4,4]{0,2,1:T(4,128)}, f32[128,4,4]{0,2,1:T(4,128)S(1)}, u32[]{:S(2)}) copy-start(f32[128,4,4]{0,2,1:T(4,128)S(1)} %rev.20) | copy-start | bytes 24580
  33.3 1.9 %copy-start.12 = (f32[1,2048]{1,0:T(1,128)S(1)}, f32[1,2048]{1,0:T(1,128)}, u32[]{:S(2)}) copy-start(f32[1,2048]{1,0:T(1,128)} %get-tuple-element.69) | copy-start | bytes 24580
  33.3 1.9 %copy-start.13 = (f32[1,2048]{1,0:T(1,128)S(1)}, f32[1,2048]{1,0:T(1,128)}, u32[]{:S(2)}) copy-start(f32[1,2048]{1,0:T(1,128)} %get-tuple-element.70) | copy-start | bytes 24580
  33.3 1.9 %copy-start.14 = (f32[1,2048]{1,0:T(1,128)S(1)}, f32[1,2048]{1,0:T(1,128)}, u32[]{:S(2)}) copy-start(f32[1,2048]{1,0:T(1,128)} %get-tuple-element.71) | copy-start | bytes 24580
  33.3 1.9 %copy-start.15 = (f32[1,2048]{1,0:T(1,128)S(1)}, f32[1,2048]{1,0:T(1,128)}, u32[]{:S(2)}) copy-start(f32[1,2048]{1,0:T(1,128)} %get-tuple-element.72) | copy-start | bytes 24580
  33.4 1.9 %copy-start.16 = (f32[1,2048]{1,0:T(1,128)S(1)}, f32[1,2048]{1,0:T(1,128)}, u32[]{:S(2)}) copy-start(f32[1,2048]{1,0:T(1,128)} %get-tuple-element.73) | copy-start | bytes 24580
  39.8 1.3 copy-start.36
  39.8 1.8 %copy-start.32 = (f32[1,128,16]{1,2,0:T(8,128)S(1)}, f32[1,128,16]{1,2,0:T(8,128)}, u32[]{:S(2)}) copy-start(f32[1,128,16]{1,2,0:T(8,128)} %get-tuple-element.74) | copy-start | bytes 24580
  39.8 1.8 %copy-start.35 = (f32[4,4]{1,0:T(4,128)S(1)}, f32[4,4]{1,0:T(4,128)}, u32[]{:S(2)}) copy-start(f32[4,4]{1,0:T(4,128)} %get-tuple-element.65) | copy-start | bytes 196
  42.7 7.2 %copy-start.18 = (f32[4,2,4]{2,1,0:T(2,128)S(1)}, f32[4,2,4]{2,1,0:T(2,128)}, u32[]{:S(2)}) copy-start(f32[4,2,4]{2,1,0:T(2,128)} %copy.133) | copy-start | bytes 388
  43.0 45.1 %copy-start.24 = (f32[4,4]{1,0:T(4,128)S(1)}, f32[4,4]{1,0:T(4,128)}, u32[]{:S(2)}) copy-start(f32[4,4]{1,0:T(4,128)} %get-tuple-element.66) | copy-start | bytes 196
  44.7 44.5 %copy-start.20 = (pred[128,128]{1,0:T(8,128)(4,1)S(1)}, pred[128,128]{1,0:T(8,128)(4,1)}, u32[]{:S(2)}) copy-start(pred[128,128]{1,0:T(8,128)(4,1)} %iota_compare_fusion) | copy-start | bytes 49156
  44.8 44.5 %copy-start.26 = (f32[128,4,4]{0,2,1:T(4,128)S(1)}, f32[128,4,4]{0,2,1:T(4,128)}, u32[]{:S(2)}) copy-start(f32[128,4,4]{0,2,1:T(4,128)} %copy.140) | copy-start | bytes 24580
  44.8 44.5 %copy-start.33 = (f32[1,128,16]{1,2,0:T(8,128)S(1)}, f32[1,128,16]{1,2,0:T(8,128)}, u32[]{:S(2)}) copy-start(f32[1,128,16]{1,2,0:T(8,128)} %get-tuple-element.74) | copy-start | bytes 24580
  49.8 1.0 copy-start
  89.3 1.0 copy-start.2
  89.3 1.0 copy-start.23
  89.3 1.3 copy-start.25
  89.3 1.3 copy-start.31
  90.7 1.0 copy-start.1
  91.9 1.0 copy-start.5
  91.9 1.0 copy-start.8
  91.9 1.0 copy-start.11
  92.7 0.7 copy-start.17
  92.9 1.0 copy-start.9
  92.9 1.0 copy-start.10
  93.8 0.7 copy-start.34
where the time goes:
time: 149 us; the launch traced here: 148 us
  Pallas kernels  86.8 us (58%)
  local copies, waits for them, and re-layouts  21.3 us (14%)
  other arithmetic  17.6 us (12%)
  starting transfers between devices  14.4 us (10%)
  matrix products  4.35 us (3%)
  waiting for transfers between devices  2.67 us (2%)
    pallas_call x1, Pallas kernels, project(): pl.pallas_call(functools.partial(project_kernel, clique, outer, tps), out...  49.7 us
    pallas_call x1, Pallas kernels, scan_states(): pl.pallas_call(functools.partial(scan_kernel, clique, outer), out_shape=(...  37.2 us
    ppermute x2, starting transfers between devices, padded_2(): lax.ppermute(tail, axis, [(i, (i + 1) % count) for i in range(ends)])  8.55 us
    convert_element_type x1, other arithmetic, convolve(): return jax.nn.silu(summed).astype(jnp.bfloat16)  4.47 us
    slice x4, local copies, waits for them, and re-layouts, banded(): return jnp.concatenate([stacked[:-2], stacked[1:-1], stacked[2:]], axis=1)  4.14 us
    unnamed x85, local copies, waits for them, and re-layouts  3.82 us
    ppermute x1, starting transfers between devices, ring_weights(): held = held + [lax.ppermute(held[-1], 'sp', pairs)]  3.29 us
  transfers between devices with their start and end apart: 5, of which 1 were waited for; matrix products, arithmetic and copies ran while one was open for 20% of the time, Pallas kernels for 0%

commit v1 on v0

v1 whole, which is shorter than its diff:
```python
import functools

import jax
import jax.numpy as jnp
from jax import lax
from jax.experimental import pallas as pl
from jax.experimental.pallas import tpu as pltpu
from jax.sharding import PartitionSpec as P

HEAD = 128
SSD_HEAD = 64
STATE = 128
CONV = 5
WINDOW = 128
CLIQUE = 4
TILE = 16
LANES = 128
CHUNKS = 4
PARTS = 4
EARLY = 3

ROTARY_BASE = 500000.0
EPSILON = 1e-06

F32 = jnp.float32
BF16 = jnp.bfloat16


def sending(source, target, send_sem, recv_sem, partner):
    return pltpu.make_async_remote_copy(
        src_ref=source,
        dst_ref=target,
        send_sem=send_sem,
        recv_sem=recv_sem,
        device_id=partner,
        device_id_type=pl.DeviceIdType.MESH,
    )


def dot(a, b):
    return jnp.dot(a, b, preferred_element_type=F32)


def dot_t(a, b):
    return lax.dot_general(a, b, (((1,), (1,)), ((), ())), preferred_element_type=F32)


def iota(shape, axis):
    return lax.broadcasted_iota(jnp.int32, shape, axis)


def silu(v):
    return v / (1.0 + jnp.exp(-v))


def split(value):
    high = value.astype(BF16)
    return high, (value - high.astype(F32)).astype(BF16)


def mixer_kernel(
    outer,
    tps,
    q_ref,
    k_ref,
    v_ref,
    gate_ref,
    src_ref,
    wr_ref,
    rd_ref,
    src_taps,
    wr_taps,
    rd_taps,
    inc_ref,
    fade_ref,
    spike_ref,
    sink_ref,
    gain_ref,
    weight_ref,
    cos_ref,
    sin_ref,
    out_ref,
    turned,
    k_halo,
    v_halo,
    src_halo,
    wr_halo,
    rd_halo,
    padded,
    xs,
    wv,
    rv,
    square,
    grown,
    scaled,
    rows_log,
    logs,
    decays,
    own_state,
    state_out,
    mate_state,
    total,
    total_out,
    partner_total,
    z_out,
    z_in,
    chip_out,
    incoming,
    y_sum,
    acts,
    weights,
    acc,
    partial,
    pieces,
    summed,
    landed,
    halo_sems,
    log_sems,
    weight_sems,
    scan_sems,
    act_sems,
    own_sems,
    piece_sems,
    out_sems,
    load_sem,
):
    count = outer * CLIQUE
    rows = q_ref.shape[0]
    me = lax.axis_index("sp")
    lane = lax.axis_index("tp")
    spot = lax.rem(me, CLIQUE)
    layer = me // CLIQUE
    base = me - spot
    core = lax.rem(spot, 2)
    side_y = spot // 2
    mate = base + spot + 1 - 2 * core
    partner = base + lax.rem(spot + 2, CLIQUE)
    across = base + CLIQUE - 1 - spot
    way = 1 - core
    step = 1 - 2 * way
    before = layer - step
    after = layer + step
    has_before = (before >= 0) & (before < outer)
    has_after = (after >= 0) & (after < outer)
    later = (side_y + way) == 1
    has_left = me > 0
    has_right = me < count - 1
    left = {"sp": me - 1}
    right = {"sp": me + 1}

    def at_layer(other):
        return {"sp": other * CLIQUE + spot}

    barrier = pltpu.get_barrier_semaphore()

    def hail(who):
        pl.semaphore_signal(
            barrier, inc=1, device_id=who, device_id_type=pl.DeviceIdType.MESH
        )

    for other in (mate, partner, across):
        hail({"sp": other})
    for d in range(1, outer):
        hail(at_layer(lax.rem(layer + d, outer)))
    for d in range(1, tps):
        hail({"tp": lax.rem(lane + d, tps)})
    extra_right = (spot == CLIQUE - 1) & has_right
    extra_left = (spot == 0) & has_left
    pl.when(extra_right)(lambda: hail(right))
    pl.when(extra_left)(lambda: hail(left))
    hails = CLIQUE - 1 + outer - 1 + tps - 1
    load = pltpu.make_async_copy(weight_ref, weights.at[spot], load_sem)
    load.start()

    cosine = cos_ref[...]
    sine = sin_ref[...]

    def turn(block):
        block = block.astype(F32)
        return (block * cosine + pltpu.roll(block, HEAD // 2, 1) * sine).astype(BF16)

    kv_heads = k_ref.shape[1] // HEAD
    for g in range(kv_heads):
        cols = slice(g * HEAD, (g + 1) * HEAD)
        turned[:, cols] = turn(k_ref[:, cols])

    heads = inc_ref.shape[1]
    gap = LANES // 4
    lane_at = iota((heads, rows), 1)
    eye = iota((heads, heads), 0) == iota((heads, heads), 1)
    steps = []
    runs = []
    for d in range(2):
        raw = inc_ref[d]
        length = jnp.maximum(raw, 0.0) + jnp.log1p(jnp.exp(-jnp.abs(raw)))
        rate = jnp.sum(
            jnp.where(eye, jnp.broadcast_to(jnp.exp(fade_ref[d : d + 1, :]), (heads, heads)), 0.0),
            axis=1,
            keepdims=True,
        )
        run = spike_ref[d] - rate * length
        hop = 1
        while hop < rows:
            if d == 0:
                moved = jnp.where(lane_at >= hop, pltpu.roll(run, hop, 1), 0.0)
            else:
                moved = jnp.where(lane_at < rows - hop, pltpu.roll(run, rows - hop, 1), 0.0)
            run = run + moved
            hop *= 2
        steps.append(length)
        runs.append(run)
    ends = [runs[0][:, rows - 1 : rows], runs[1][:, 0:1]]
    square[...] = jnp.zeros_like(square)
    for d in range(2):
        square[0, d * gap : d * gap + heads, :] = runs[d]
        fill = jnp.exp(runs[d])
        high = fill.astype(BF16).astype(F32)
        square[1, 2 * d * gap : 2 * d * gap + heads, :] = high
        square[1, (2 * d + 1) * gap : (2 * d + 1) * gap + heads, :] = fill - high
        fill = steps[d] * jnp.exp(ends[d] - runs[d])
        high = fill.astype(BF16).astype(F32)
        square[2, 2 * d * gap : 2 * d * gap + heads, :] = high
        square[2, (2 * d + 1) * gap : (2 * d + 1) * gap + heads, :] = fill - high
        rows_log[d] = runs[d]
        rows_log[2 + d] = steps[d]
    run_cols = square[0].T
    log_row = iota((8, LANES), 0)
    logs[spot] = jnp.where(
        log_row == 0,
        jnp.broadcast_to(run_cols[rows - 1 : rows, :], (8, LANES)),
        jnp.broadcast_to(run_cols[0:1, :], (8, LANES)),
    )

    def when_wait(ready):
        pl.semaphore_wait(barrier, ready)

    when_wait(
        hails + extra_right.astype(jnp.int32) + extra_left.astype(jnp.int32)
    )

    rims = (
        (src_ref, src_halo, TILE),
        (wr_ref, wr_halo, TILE),
        (rd_ref, rd_halo, TILE),
        (turned, k_halo, rows),
        (v_ref, v_halo, rows),
    )

    def rim_copy(index, to_right):
        source, target, depth = rims[index]
        side = 0 if to_right else 1
        first = rows - depth if to_right else 0
        return sending(
            source.at[first : first + depth, :],
            target.at[side],
            halo_sems.at[0, side, index],
            halo_sems.at[1, side, index],
            right if to_right else left,
        )

    def rims_do(indices, what):
        for index in indices:
            if what == "start":
                pl.when(has_right)(lambda: rim_copy(index, True).start())
                pl.when(has_left)(lambda: rim_copy(index, False).start())
            elif what == "recv":
                pl.when(has_left)(lambda: rim_copy(index, True).wait_recv())
                pl.when(has_right)(lambda: rim_copy(index, False).wait_recv())
            else:
                pl.when(has_right)(lambda: rim_copy(index, True).wait_send())
                pl.when(has_left)(lambda: rim_copy(index, False).wait_send())

    rims_do(range(5), "start")

    def clear(side):
        for _, target, _ in rims:
            target[side] = jnp.zeros(target.shape[1:], target.dtype)

    pl.when(jnp.logical_not(has_left))(lambda: clear(0))
    pl.when(jnp.logical_not(has_right))(lambda: clear(1))

    def clear_in():
        z_in[...] = jnp.zeros_like(z_in)

    pl.when(jnp.logical_not(has_before))(clear_in)

    def log_copy(flip, who, slot):
        return sending(
            logs.at[slot],
            logs.at[slot],
            log_sems.at[0, flip],
            log_sems.at[1, flip],
            {"sp": base + who},
        )

    flips = (
        spot + 1 - 2 * core,
        lax.rem(spot + 2, CLIQUE),
        CLIQUE - 1 - spot,
    )
    for flip, who in enumerate(flips):
        log_copy(flip, who, spot).start()

    load.wait()
    depth = weights.shape[2] // PARTS

    def weight_part(slot, index):
        half, part = divmod(index, PARTS)
        return weights.at[slot, half, part * depth : (part + 1) * depth, :]

    def weight_mate(half, slot):
        return sending(
            weights.at[slot, half],
            weights.at[slot, half],
            weight_sems.at[0, 0, half],
            weight_sems.at[1, 0, half],
            {"sp": mate},
        )

    def weight_over(index, slot):
        return sending(
            weight_part(slot, index),
            weight_part(slot, index),
            weight_sems.at[0, 1, index],
            weight_sems.at[1, 1, index],
            {"sp": partner},
        )

    def weight_onward(index, slot):
        return sending(
            weight_part(slot, index),
            weight_part(slot, index),
            weight_sems.at[0, 2, index],
            weight_sems.at[1, 2, index],
            {"sp": mate},
        )

    def pass_on(index):
        weight_over(index, flips[1]).wait_recv()
        weight_onward(index, flips[1]).start()

    for index in range(EARLY):
        weight_over(index, spot).start()
    for half in range(2):
        weight_mate(half, spot).start()

    rims_do(range(3), "recv")
    columns = ((src_ref, src_halo, src_taps, xs), (wr_ref, wr_halo, wr_taps, wv), (rd_ref, rd_halo, rd_taps, rv))
    margin = CONV // 2
    for source, halo, taps_ref, target in columns:
        width = source.shape[1]
        taps = taps_ref[...].astype(F32)
        for first in range(0, width, LANES):
            cols = slice(first, first + LANES)
            padded[8 : 8 + rows, :] = source[:, cols].astype(F32)
            padded[0:8, :] = halo[0, TILE // 2 :, cols].astype(F32)
            padded[8 + rows : 16 + rows, :] = halo[1, : TILE // 2, cols].astype(F32)
            value = jnp.zeros((rows, LANES), F32)
            for k in range(CONV):
                start = 8 - margin + k
                value = value + padded[start : start + rows, :] * taps[k : k + 1, cols]
            target[:, cols] = silu(value).astype(BF16)

    rims_do(range(3, 5), "recv")
    sharing = q_ref.shape[1] // HEAD // kv_heads
    above = iota((rows, rows), 1) >= iota((rows, rows), 0)
    below = iota((rows, rows), 1) <= iota((rows, rows), 0)
    ok_left = above & has_left
    ok_right = below & has_right
    scale = HEAD ** (-0.5)
    for g in range(kv_heads):
        cols = slice(g * HEAD, (g + 1) * HEAD)
        keys = (k_halo[0, :, cols], turned[:, cols], k_halo[1, :, cols])
        values = (v_halo[0, :, cols], v_ref[:, cols], v_halo[1, :, cols])
        for j in range(sharing):
            h = g * sharing + j
            mine = slice(h * HEAD, (h + 1) * HEAD)
            query = turn(q_ref[:, mine])
            tiles = [dot_t(query, key) * scale for key in keys]
            tiles[0] = jnp.where(ok_left, tiles[0], -jnp.inf)
            tiles[2] = jnp.where(ok_right, tiles[2], -jnp.inf)
            sink = sink_ref[h]
            top = jnp.maximum(
                jnp.max(
                    jnp.maximum(jnp.maximum(tiles[0], tiles[1]), tiles[2]), axis=1, keepdims=True
                ),
                sink,
            )
            tiles = [jnp.exp(tile - top) for tile in tiles]
            bottom = jnp.sum(tiles[0] + tiles[1] + tiles[2], axis=1, keepdims=True) + jnp.exp(
                sink - top
            )
            found = jnp.zeros((rows, HEAD), F32)
            for tile, value in zip(tiles, values):
                found = found + dot((tile / bottom).astype(BF16), value)
            acts[0, layer, :, mine] = found.astype(BF16)

    def own_copy(half, way_up):
        target = layer + (1 if way_up else -1)
        return sending(
            acts.at[half, layer],
            acts.at[half, layer],
            own_sems.at[half, 1 if way_up else 0],
            act_sems.at[1, half, layer],
            at_layer(target),
        )

    can_up = layer < outer - 1
    can_down = layer > 0

    def own_start(half):
        pl.when(can_up)(lambda: own_copy(half, True).start())
        pl.when(can_down)(lambda: own_copy(half, False).start())

    def far_copy(half, block, sign):
        return sending(
            acts.at[half, block],
            acts.at[half, block],
            act_sems.at[0, half, block],
            act_sems.at[1, half, block],
            at_layer(layer - sign),
        )

    def each(d, do):
        for sign in (-1, 1):
            block = layer + sign * d
            pl.when((block >= 0) & (block < outer))(functools.partial(do, block, sign))

    def relay(half, d):
        def do(block, sign):
            copy = far_copy(half, block, sign)
            copy.wait_recv()
            target = layer - sign
            pl.when((target >= 0) & (target < outer))(lambda: copy.start())

        each(d, do)

    own_start(0)

    groups = wr_ref.shape[1] // STATE
    wide = xs.shape[1]
    group_wide = wide // groups
    per_group = group_wide // SSD_HEAD
    owner = iota((LANES, wide), 1) // SSD_HEAD
    place = iota((LANES, wide), 0)
    pick = []
    for d in range(2):
        hit = (place == owner + 2 * d * gap) | (place == owner + (2 * d + 1) * gap)
        pick.append(jnp.where(hit, 1.0, 0.0).astype(BF16))
    grow_cols = square[1].T.astype(BF16)
    scale_cols = square[2].T.astype(BF16)
    for d in range(2):
        grown[d] = dot(grow_cols, pick[d])
        scaled[d] = (dot(scale_cols, pick[d]) * xs[...].astype(F32)).astype(BF16)
    for g in range(groups):
        cols = slice(g * group_wide, (g + 1) * group_wide)
        write_t = wv[:, g * STATE : (g + 1) * STATE].astype(F32).T.astype(BF16)
        for d in range(2):
            fresh = dot(write_t, scaled[d, :, cols])
            own_state[d, :, cols] = fresh
            state_out[d, :, cols] = fresh.astype(BF16)

    swap = sending(
        state_out.at[1 - way],
        mate_state,
        scan_sems.at[0, 0, 0],
        scan_sems.at[1, 0, 0],
        {"sp": mate},
    )
    swap.start()

    for flip, who in enumerate(flips):
        log_copy(flip, who, who).wait_recv()
    log_own = logs[spot, pl.ds(way, 1), :]
    log_mate = logs[flips[0], pl.ds(way, 1), :]
    log_partner = logs[flips[1], pl.ds(way, 1), :] + logs[flips[2], pl.ds(way, 1), :]
    log_rows = jnp.where(
        log_row == 0,
        jnp.broadcast_to(log_own, (8, LANES)),
        jnp.where(
            log_row == 1,
            jnp.broadcast_to(log_mate, (8, LANES)),
            jnp.where(
                log_row == 2,
                jnp.broadcast_to(log_partner, (8, LANES)),
                jnp.broadcast_to(log_own + log_mate, (8, LANES)),
            ),
        ),
    )
    high, low = split(jnp.exp(log_rows))
    mine = jnp.where(place == owner + way * gap, 1.0, 0.0).astype(BF16)
    decays[...] = dot(high, mine) + dot(low, mine)
    dec_own = decays[0:1, :]
    dec_mate = decays[1:2, :]
    dec_partner = decays[2:3, :]
    dec_chip = decays[3:4, :]
    dec_layer = dec_partner * dec_chip
    one = jnp.ones_like(dec_own)
    from_partner = jnp.where(later, dec_chip, one)
    from_mine = jnp.where(later, one, dec_partner)
    in_before = jnp.where(later, dec_partner, one)
    in_partner = jnp.where(later, 1.0, 0.0)

    chunk = STATE // CHUNKS

    def over_copy(c):
        part = slice(c * chunk, (c + 1) * chunk)
        return sending(
            total_out.at[part, :],
            partner_total.at[part, :],
            scan_sems.at[0, 1, c],
            scan_sems.at[1, 1, c],
            {"sp": partner},
        )

    def z_copy(c, to):
        part = slice(c * chunk, (c + 1) * chunk)
        return sending(
            z_out.at[part, :],
            z_in.at[part, :],
            scan_sems.at[0, 2, c],
            scan_sems.at[1, 2, c],
            at_layer(to),
        )

    def down_copy(c):
        part = slice(c * chunk, (c + 1) * chunk)
        return sending(
            chip_out.at[part, :],
            incoming.at[way, part, :],
            scan_sems.at[0, 3, c],
            scan_sems.at[1, 3, c],
            {"sp": mate},
        )

    def down_recv(c):
        part = slice(c * chunk, (c + 1) * chunk)
        return sending(
            chip_out.at[part, :],
            incoming.at[1 - way, part, :],
            scan_sems.at[0, 3, c],
            scan_sems.at[1, 3, c],
            {"sp": mate},
        )

    swap.wait_recv()
    for c in range(CHUNKS):
        part = slice(c * chunk, (c + 1) * chunk)
        summed_state = (
            mate_state[part, :].astype(F32) * dec_own + own_state[way, part, :]
        )
        total[part, :] = summed_state
        total_out[part, :] = summed_state.astype(BF16)
        over_copy(c).start()
    for index in range(EARLY, 2 * PARTS):
        weight_over(index, spot).start()

    run_at = square[0].T
    causal = iota((rows, rows), 1) <= iota((rows, rows), 0)
    diagonal = iota((rows, rows), 1) == iota((rows, rows), 0)

    def within(g):
        read = rv[:, g * STATE : (g + 1) * STATE]
        write = wv[:, g * STATE : (g + 1) * STATE]
        affinity = dot_t(read, write)
        for j in range(per_group):
            h = g * per_group + j
            cols = slice(h * SSD_HEAD, (h + 1) * SSD_HEAD)
            ahead = run_at[:, h : h + 1] - rows_log[0, h : h + 1, :]
            back = run_at[:, gap + h : gap + h + 1] - rows_log[1, h : h + 1, :]
            fade = jnp.exp(jnp.where(causal, ahead, back))
            length_f = rows_log[2, h : h + 1, :]
            length_b = rows_log[3, h : h + 1, :]
            taken = jnp.where(causal, length_f, length_b) * fade
            taken = taken + jnp.where(diagonal, length_b, 0.0)
            y_sum[:, cols] = dot((affinity * taken).astype(BF16), xs[:, cols])

    for g in range(groups):
        within(g)
    for index in range(EARLY):
        pass_on(index)

    for c in range(CHUNKS):
        part = slice(c * chunk, (c + 1) * chunk)
        over_copy(c).wait_recv()
        theirs = partner_total[part, :].astype(F32)
        level = theirs * from_partner + total[part, :] * from_mine
        pl.when(has_before)(lambda: z_copy(c, after).wait_recv())
        entering = z_in[part, :].astype(F32)
        z_out[part, :] = (entering * dec_layer + level).astype(BF16)
        pl.when(has_after)(lambda: z_copy(c, after).start())
        chip_in = entering * in_before + theirs * in_partner
        chip_out[part, :] = chip_in.astype(BF16)
        down_copy(c).start()
        incoming[way, part, :] = (
            chip_in * dec_mate + mate_state[part, :].astype(F32)
        ).astype(BF16)
    if outer > 1:
        relay(0, 1)
    for c in range(CHUNKS):
        down_recv(c).wait_recv()

    for g in range(groups):
        cols = slice(g * group_wide, (g + 1) * group_wide)
        read = rv[:, g * STATE : (g + 1) * STATE]
        value = y_sum[:, cols]
        for d in range(2):
            value = value + dot(read, incoming[d, :, cols]) * grown[d, :, cols]
        value = value * silu(gate_ref[:, cols].astype(F32))
        mean = jnp.sum(value * value, axis=1, keepdims=True) * (1.0 / group_wide)
        value = value * lax.rsqrt(mean + EPSILON) * gain_ref[:, cols]
        acts[1, layer, :, cols] = value.astype(BF16)
    own_start(1)

    share = rows // tps

    def multiply_first(block, sign):
        def body(slot, carry):
            acc[block, slot] = dot(acts[0, block], weights[slot, 0])
            return carry

        lax.fori_loop(0, CLIQUE, body, 0)

    def piece_copy(block, other, slot):
        return sending(
            partial.at[block, other],
            pieces.at[block, slot],
            piece_sems.at[0, block, other],
            piece_sems.at[1, block, slot],
            {"tp": other},
        )

    lanes = [lax.rem(lane + d, tps) for d in range(1, tps)]

    def multiply_second(block, sign):
        def body(slot, carry):
            product = (acc[block, slot] + dot(acts[1, block], weights[slot, 1])).astype(BF16)
            for other in range(tps):
                partial[block, other, slot] = product[other * share : (other + 1) * share]
            return carry

        lax.fori_loop(0, CLIQUE, body, 0)
        for other in lanes:
            piece_copy(block, other, lane).start()

    def out_copy(block, slot):
        return sending(
            summed.at[block],
            landed.at[slot],
            out_sems.at[0, block],
            out_sems.at[1, slot],
            at_layer(block),
        )

    def settle(block, sign):
        result = partial[block, lane].astype(F32)
        for other in lanes:
            piece_copy(block, other, other).wait_recv()
            result = result + pieces[block, other].astype(F32)
        if sign:
            summed[block] = result.astype(BF16)
            out_copy(block, layer).start()
        else:
            landed[layer] = result.astype(BF16)

    for index in range(EARLY, PARTS):
        pass_on(index)
    weight_mate(0, flips[0]).wait_recv()
    for index in range(PARTS):
        weight_onward(index, flips[2]).wait_recv()
    multiply_first(layer, 0)
    for d in range(1, outer):
        if d > 1:
            relay(0, d)
        each(d, multiply_first)
    for index in range(PARTS, 2 * PARTS):
        pass_on(index)
    weight_mate(1, flips[0]).wait_recv()
    for index in range(PARTS, 2 * PARTS):
        weight_onward(index, flips[2]).wait_recv()
    multiply_second(layer, 0)
    for d in range(1, outer):
        relay(1, d)
        each(d, multiply_second)
        if d == 1:
            settle(layer, 0)
        else:
            each(d - 1, settle)
    if outer > 1:
        each(outer - 1, settle)
    else:
        settle(layer, 0)

    def arrive(block, sign):
        out_copy(block, block).wait_recv()

    for d in range(1, outer):
        each(d, arrive)
    width = landed.shape[3]
    for other in range(outer):
        for slot in range(CLIQUE):
            first = (other * CLIQUE + slot) * width
            out_ref[:, first : first + width] = landed[other, slot]

    rims_do(range(5), "send")
    for flip, who in enumerate(flips):
        log_copy(flip, who, spot).wait_send()
    for half in range(2):
        weight_mate(half, spot).wait_send()
        pl.when(can_up)(lambda: own_copy(half, True).wait_send())
        pl.when(can_down)(lambda: own_copy(half, False).wait_send())
    for index in range(2 * PARTS):
        weight_over(index, spot).wait_send()
        weight_onward(index, flips[1]).wait_send()
    swap.wait_send()
    for c in range(CHUNKS):
        over_copy(c).wait_send()
        down_copy(c).wait_send()
        pl.when(has_after)(lambda: z_copy(c, after).wait_send())

    def gone(block, sign):
        target = layer - sign
        for half in range(2):
            pl.when((target >= 0) & (target < outer))(
                lambda: far_copy(half, block, sign).wait_send()
            )
        out_copy(block, layer).wait_send()
        for other in lanes:
            piece_copy(block, other, lane).wait_send()

    for d in range(1, outer):
        each(d, gone)
    for other in lanes:
        piece_copy(layer, other, lane).wait_send()


def local(
    asking_matrix,
    matching_key_matrix,
    carried_value_matrix,
    silu_switch_argument,
    duality_source_matrix,
    storing_direction_matrix,
    fetching_direction_matrix,
    duality_kernel_coefficients,
    storing_kernel_coefficients,
    fetching_kernel_coefficients,
    raw_increment_lengths,
    logarithmic_fading_speeds,
    token_fading_spikes,
    absorber_score_vector,
    cluster_scaling_factor,
    final_mapping_matrix,
):
    count = lax.axis_size("sp")
    tps = lax.axis_size("tp")
    outer = count // CLIQUE
    rows, q_width = asking_matrix.shape
    k_width = matching_key_matrix.shape[1]
    s_width = duality_source_matrix.shape[1]
    w_width = storing_direction_matrix.shape[1]
    heads = raw_increment_lengths.shape[1]
    width = final_mapping_matrix.shape[2]
    share = rows // tps
    halfway = HEAD // 2
    spacing = ROTARY_BASE ** (-jnp.arange(halfway, dtype=F32) * 2.0 / HEAD)
    places = (lax.axis_index("sp") * rows + jnp.arange(rows, dtype=jnp.int32)).astype(F32)
    angles = places[:, None] * jnp.concatenate([spacing, spacing])[None, :]
    sign = jnp.where(jnp.arange(HEAD) < halfway, -1.0, 1.0).astype(F32)
    cosine = jnp.cos(angles)
    sine = jnp.sin(angles) * sign[None, :]
    vmem = pl.BlockSpec(memory_space=pltpu.VMEM)
    block = (CLIQUE, share, width)
    return pl.pallas_call(
        functools.partial(mixer_kernel, outer, tps),
        out_shape=jax.ShapeDtypeStruct((share, count * width), BF16),
        in_specs=[vmem] * 13
        + [pl.BlockSpec(memory_space=pltpu.SMEM), vmem, pl.BlockSpec(memory_space=pl.ANY)]
        + [vmem] * 2,
        out_specs=vmem,
        scratch_shapes=[
            pltpu.VMEM((rows, k_width), BF16),
            pltpu.VMEM((2, rows, k_width), BF16),
            pltpu.VMEM((2, rows, k_width), BF16),
            pltpu.VMEM((2, TILE, s_width), BF16),
            pltpu.VMEM((2, TILE, w_width), BF16),
            pltpu.VMEM((2, TILE, w_width), BF16),
            pltpu.VMEM((rows + 16, LANES), F32),
            pltpu.VMEM((rows, s_width), BF16),
            pltpu.VMEM((rows, w_width), BF16),
            pltpu.VMEM((rows, w_width), BF16),
            pltpu.VMEM((3, LANES, rows), F32),
            pltpu.VMEM((2, rows, s_width), F32),
            pltpu.VMEM((2, rows, s_width), BF16),
            pltpu.VMEM((4, heads, rows), F32),
            pltpu.VMEM((CLIQUE, 8, LANES), F32),
            pltpu.VMEM((8, s_width), F32),
            pltpu.VMEM((2, STATE, s_width), F32),
            pltpu.VMEM((2, STATE, s_width), BF16),
            pltpu.VMEM((STATE, s_width), BF16),
            pltpu.VMEM((STATE, s_width), F32),
            pltpu.VMEM((STATE, s_width), BF16),
            pltpu.VMEM((STATE, s_width), BF16),
            pltpu.VMEM((STATE, s_width), BF16),
            pltpu.VMEM((STATE, s_width), BF16),
            pltpu.VMEM((STATE, s_width), BF16),
            pltpu.VMEM((2, STATE, s_width), BF16),
            pltpu.VMEM((rows, s_width), F32),
            pltpu.VMEM((2, outer, rows, q_width), BF16),
            pltpu.VMEM((CLIQUE,) + final_mapping_matrix.shape, BF16),
            pltpu.VMEM((outer, CLIQUE, rows, width), F32),
            pltpu.VMEM((outer, tps) + block, BF16),
            pltpu.VMEM((outer, tps) + block, BF16),
            pltpu.VMEM((outer,) + block, BF16),
            pltpu.VMEM((outer,) + block, BF16),
            pltpu.SemaphoreType.DMA((2, 2, 5)),
            pltpu.SemaphoreType.DMA((2, CLIQUE)),
            pltpu.SemaphoreType.DMA((2, 3, 2 * PARTS)),
            pltpu.SemaphoreType.DMA((2, 4, CHUNKS)),
            pltpu.SemaphoreType.DMA((2, 2, outer)),
            pltpu.SemaphoreType.DMA((2, 2)),
            pltpu.SemaphoreType.DMA((2, outer, tps)),
            pltpu.SemaphoreType.DMA((2, outer)),
            pltpu.SemaphoreType.DMA,
        ],
        compiler_params=pltpu.CompilerParams(collective_id=1, has_side_effects=True),
    )(
        asking_matrix,
        matching_key_matrix,
        carried_value_matrix,
        silu_switch_argument,
        duality_source_matrix,
        storing_direction_matrix,
        fetching_direction_matrix,
        duality_kernel_coefficients,
        storing_kernel_coefficients,
        fetching_kernel_coefficients,
        raw_increment_lengths,
        logarithmic_fading_speeds,
        token_fading_spikes,
        absorber_score_vector,
        cluster_scaling_factor.reshape(1, s_width),
        final_mapping_matrix,
        cosine,
        sine,
    )


def solution(mesh):
    in_specs = (
        P("sp", "tp"),
        P("sp", "tp"),
        P("sp", "tp"),
        P("sp", "tp"),
        P("sp", "tp"),
        P("sp", "tp"),
        P("sp", "tp"),
        P(None, "tp"),
        P(None, "tp"),
        P(None, "tp"),
        P(None, "tp", "sp"),
        P(None, "tp"),
        P(None, "tp", "sp"),
        P("tp"),
        P("tp"),
        P(None, "tp", "sp"),
    )
    out_specs = P(("sp", "tp"), None)
    return jax.shard_map(local, mesh=mesh, in_specs=in_specs, out_specs=out_specs, check_vma=False)
```

time: 149 us -> 86.1 us (0.58)
  local copies, waits for them, and re-layouts: 21.3 us -> 1.87 us
  other arithmetic: 17.6 us -> 1.06 us
  starting transfers between devices: 14.4 us -> 0 us
  matrix products: 4.35 us -> 0 us
  Pallas kernels: 86.8 us -> 83 us
  waiting for transfers between devices: 2.67 us -> 0 us
    ppermute x5 -> x0, starting transfers between devices: 14.4 us -> none  [the longest x2 8.55 us: padded_2(): lax.ppermute(tail, axis, [(i, (i + 1) % count) for i in range(ends)])]
    slice x9 -> x0, local copies, waits for them, and re-layouts: 6.09 us -> none  [the longest x4 4.14 us: banded(): return jnp.concatenate([stacked[:-2], stacked[1:-1], stacked[2:]], axis=1)]
    convert_element_type x4 -> x1, other arithmetic: 5.33 us -> 0.01 us  [local(): (lax.axis_index('sp') * rows + jnp.arange(rows, dtype=jnp.int32)).astype(...]
    dot_general x10 -> x0, matrix products: 4.35 us -> none  [the longest x2 1.51 us: finish(): jnp.einsum('blgn,bgrpn->blgrp', read_tiles.astype(jnp.float32), starting)]
    pallas_call x2 -> x1, Pallas kernels: 86.8 us -> 83 us  [local(): pl.pallas_call(functools.partial(mixer_kernel, outer, tps), out_shape=jax...]
    another operation x6 -> x0, other arithmetic: 3.7 us -> none  [the longest x1 1.64 us: rotate(): jnp.stack([former * cosine - latter * sine_table, latter * cosine + forme...]
    ppermute x5 -> x0, waiting for transfers between devices: 2.67 us -> none  [the longest x1 2.66 us: ring_weights(): held = held + [lax.ppermute(held[-1], 'sp', pairs)]]
    concatenate x3 -> x0, other arithmetic: 2.6 us -> none  [the longest x1 1.84 us: padded_2(): jnp.concatenate([lax.ppermute(tail, axis, [(i, (i + 1) % count) for i in...]
  transfers between devices with their start and end apart: 5 -> 0, of which waited for: 1 -> 0; matrix products, arithmetic and copies ran while one was open for 20% -> 0% of each run, Pallas kernels for 0% -> 0%
where the time goes in v1:
time: 86.1 us; the launch traced here: 85.9 us
  Pallas kernels  83 us (96%)
  local copies, waits for them, and re-layouts  1.87 us (2%)
  other arithmetic  1.06 us (1%)
    pallas_call x1, Pallas kernels, local(): pl.pallas_call(functools.partial(mixer_kernel, outer, tps), out_shape=jax...  83 us
    unnamed x1, local copies, waits for them, and re-layouts  1.87 us

profile of v1, /device:TPU:0, one launch (start us, length us, event | category | flops | bytes accessed | tf_op | source)
XLA Modules:
  0.0 85.9 jit_solution(18232166733174859007)
XLA Ops:
  0.0 0.1 compare_select_fusion
  0.1 1.0 %fusion = (f32[128,128]{1,0:T(8,128)}, f32[128,128]{1,0:T(8,128)}) fusion(f32[128]{0:T(128)S(1)} %get-tuple-element.7, f32[128]{0:T(128)S(1)} %get-tuple-element.8, f32[128]{0:T(128)S(1)} %add_convert_fusion), kind=kLoop, calls=%fused_computation.2 | loop fusion | flops 32768 | bytes 132608 | tf_op jit(solution)/shard_map/mul | solution.py:771
  1.1 83.0 %shard_map.154 = bf16[64,4096]{1,0:T(8,128)(2,1)} custom-call(bf16[128,1024]{1,0:T(8,128)(2,1)} %q_ref.1, bf16[128,512]{1,0:T(8,128)(2,1)} %k_ref.1, bf16[128,512]{1,0:T(8,128)(2,1)} %v_ref.1, bf16[128,1024]{1,0:T(8,128)(2,1)} %gate_ref.1, bf16[128,1024]{1,0:T(8,128)(2,1)} %src_ref.1, bf16[128,512]{1,0:T(8,128)(2,1)} %wr_ref.1, bf16[128,512]{1,0:T(8,128)(2,1)} %rd_ref.1, ...), custom_call_target="tpu_custom_call" | custom-call | tf_op jit(solution)/shard_map/pallas_call | solution.py:774
  84.1 1.9 %copy.18 = bf16[64,4096]{1,0:T(8,128)(2,1)} copy(bf16[64,4096]{1,0:T(8,128)(2,1)} %shard_map.154) | data formatting | bytes 1048576
  (2 shorter events, 0.0 us)

commit v2 on v1

--- a/solution.py
+++ b/solution.py
@@ -2,6 +2,7 @@
 
 import jax
 import jax.numpy as jnp
+import numpy as np
 from jax import lax
 from jax.experimental import pallas as pl
 from jax.experimental.pallas import tpu as pltpu
@@ -13,11 +14,11 @@
 CONV = 5
 WINDOW = 128
 CLIQUE = 4
-TILE = 16
+TILE = 8
 LANES = 128
 CHUNKS = 4
 PARTS = 4
-EARLY = 3
+SPLIT = 2
 
 ROTARY_BASE = 500000.0
 EPSILON = 1e-06
@@ -61,6 +62,26 @@
 def mixer_kernel(
     outer,
     tps,
+    q_hbm,
+    k_hbm,
+    v_hbm,
+    gate_hbm,
+    src_hbm,
+    wr_hbm,
+    rd_hbm,
+    src_taps_hbm,
+    wr_taps_hbm,
+    rd_taps_hbm,
+    inc_hbm,
+    fade_hbm,
+    spike_hbm,
+    sink_hbm,
+    gain_hbm,
+    weight_hbm,
+    cos_hbm,
+    sin_hbm,
+    base_hbm,
+    out_ref,
     q_ref,
     k_ref,
     v_ref,
@@ -76,10 +97,9 @@
     spike_ref,
     sink_ref,
     gain_ref,
-    weight_ref,
     cos_ref,
     sin_ref,
-    out_ref,
+    base_ref,
     turned,
     k_halo,
     v_halo,
@@ -122,7 +142,7 @@
     own_sems,
     piece_sems,
     out_sems,
-    load_sem,
+    load_sems,
 ):
     count = outer * CLIQUE
     rows = q_ref.shape[0]
@@ -151,6 +171,34 @@
     def at_layer(other):
         return {"sp": other * CLIQUE + spot}
 
+    loads = [
+        pltpu.make_async_copy(source, target, load_sems.at[index])
+        for index, (source, target) in enumerate(
+            (
+                (base_hbm, base_ref),
+                (src_hbm, src_ref),
+                (wr_hbm, wr_ref),
+                (rd_hbm, rd_ref),
+                (k_hbm, k_ref),
+                (cos_hbm, cos_ref),
+                (sin_hbm, sin_ref),
+                (inc_hbm, inc_ref),
+                (fade_hbm, fade_ref),
+                (spike_hbm, spike_ref),
+                (src_taps_hbm, src_taps),
+                (wr_taps_hbm, wr_taps),
+                (rd_taps_hbm, rd_taps),
+                (v_hbm, v_ref),
+                (q_hbm, q_ref),
+                (sink_hbm, sink_ref),
+                (weight_hbm, weights.at[spot]),
+                (gate_hbm, gate_ref),
+                (gain_hbm, gain_ref),
+            )
+        )
+    ]
+    for load in loads:
+        load.start()
     barrier = pltpu.get_barrier_semaphore()
 
     def hail(who):
@@ -169,11 +217,69 @@
     pl.when(extra_right)(lambda: hail(right))
     pl.when(extra_left)(lambda: hail(left))
     hails = CLIQUE - 1 + outer - 1 + tps - 1
-    load = pltpu.make_async_copy(weight_ref, weights.at[spot], load_sem)
-    load.start()
-
-    cosine = cos_ref[...]
-    sine = sin_ref[...]
+
+    def loaded(*indices):
+        for index in indices:
+            loads[index].wait()
+
+
+    loaded(1, 2, 3)
+    pl.semaphore_wait(
+        barrier, hails + extra_right.astype(jnp.int32) + extra_left.astype(jnp.int32)
+    )
+
+    rims = (
+        (src_ref, src_halo, TILE),
+        (wr_ref, wr_halo, TILE),
+        (rd_ref, rd_halo, TILE),
+        (turned, k_halo, rows),
+        (v_ref, v_halo, rows),
+    )
+
+    def rim_copy(index, to_right):
+        source, target, depth = rims[index]
+        side = 0 if to_right else 1
+        first = rows - depth if to_right else 0
+        return sending(
+            source.at[first : first + depth, :],
+            target.at[side],
+            halo_sems.at[0, side, index],
+            halo_sems.at[1, side, index],
+            right if to_right else left,
+        )
+
+    def rims_do(indices, what):
+        for index in indices:
+            if what == "start":
+                pl.when(has_right)(lambda: rim_copy(index, True).start())
+                pl.when(has_left)(lambda: rim_copy(index, False).start())
+            elif what == "recv":
+                pl.when(has_left)(lambda: rim_copy(index, True).wait_recv())
+                pl.when(has_right)(lambda: rim_copy(index, False).wait_recv())
+            else:
+                pl.when(has_right)(lambda: rim_copy(index, True).wait_send())
+                pl.when(has_left)(lambda: rim_copy(index, False).wait_send())
+
+    rims_do(range(3), "start")
+
+    def clear(side):
+        for _, target, _ in rims:
+            target[side] = jnp.zeros(target.shape[1:], target.dtype)
+
+    pl.when(jnp.logical_not(has_left))(lambda: clear(0))
+    pl.when(jnp.logical_not(has_right))(lambda: clear(1))
+
+    def clear_in():
+        z_in[...] = jnp.zeros_like(z_in)
+
+    pl.when(jnp.logical_not(has_before))(clear_in)
+
+    loaded(0, 4, 5, 6)
+    base_cos = base_ref[0, pl.ds(me, 1), :]
+    base_sin = base_ref[1, pl.ds(me, 1), :]
+    cosine = base_cos * cos_ref[...] - base_sin * sin_ref[...]
+    sine = base_sin * cos_ref[...] + base_cos * sin_ref[...]
+    sine = jnp.where(iota((rows, HEAD), 1) < HEAD // 2, -sine, sine)
 
     def turn(block):
         block = block.astype(F32)
@@ -184,6 +290,7 @@
         cols = slice(g * HEAD, (g + 1) * HEAD)
         turned[:, cols] = turn(k_ref[:, cols])
 
+    loaded(7, 8, 9)
     heads = inc_ref.shape[1]
     gap = LANES // 4
     lane_at = iota((heads, rows), 1)
@@ -231,59 +338,6 @@
         jnp.broadcast_to(run_cols[0:1, :], (8, LANES)),
     )
 
-    def when_wait(ready):
-        pl.semaphore_wait(barrier, ready)
-
-    when_wait(
-        hails + extra_right.astype(jnp.int32) + extra_left.astype(jnp.int32)
-    )
-
-    rims = (
-        (src_ref, src_halo, TILE),
-        (wr_ref, wr_halo, TILE),
-        (rd_ref, rd_halo, TILE),
-        (turned, k_halo, rows),
-        (v_ref, v_halo, rows),
-    )
-
-    def rim_copy(index, to_right):
-        source, target, depth = rims[index]
-        side = 0 if to_right else 1
-        first = rows - depth if to_right else 0
-        return sending(
-            source.at[first : first + depth, :],
-            target.at[side],
-            halo_sems.at[0, side, index],
-            halo_sems.at[1, side, index],
-            right if to_right else left,
-        )
-
-    def rims_do(indices, what):
-        for index in indices:
-            if what == "start":
-                pl.when(has_right)(lambda: rim_copy(index, True).start())
-                pl.when(has_left)(lambda: rim_copy(index, False).start())
-            elif what == "recv":
-                pl.when(has_left)(lambda: rim_copy(index, True).wait_recv())
-                pl.when(has_right)(lambda: rim_copy(index, False).wait_recv())
-            else:
-                pl.when(has_right)(lambda: rim_copy(index, True).wait_send())
-                pl.when(has_left)(lambda: rim_copy(index, False).wait_send())
-
-    rims_do(range(5), "start")
-
-    def clear(side):
-        for _, target, _ in rims:
-            target[side] = jnp.zeros(target.shape[1:], target.dtype)
-
-    pl.when(jnp.logical_not(has_left))(lambda: clear(0))
-    pl.when(jnp.logical_not(has_right))(lambda: clear(1))
-
-    def clear_in():
-        z_in[...] = jnp.zeros_like(z_in)
-
-    pl.when(jnp.logical_not(has_before))(clear_in)
-
     def log_copy(flip, who, slot):
         return sending(
             logs.at[slot],
@@ -301,19 +355,20 @@
     for flip, who in enumerate(flips):
         log_copy(flip, who, spot).start()
 
-    load.wait()
-    depth = weights.shape[2] // PARTS
+    loaded(13)
+    rims_do(range(3, 5), "start")
+
+    loaded(16)
 
     def weight_part(slot, index):
-        half, part = divmod(index, PARTS)
-        return weights.at[slot, half, part * depth : (part + 1) * depth, :]
-
-    def weight_mate(half, slot):
-        return sending(
-            weights.at[slot, half],
-            weights.at[slot, half],
-            weight_sems.at[0, 0, half],
-            weight_sems.at[1, 0, half],
+        return weights.at[slot, index]
+
+    def weight_mate(slot):
+        return sending(
+            weights.at[slot],
+            weights.at[slot],
+            weight_sems.at[0, 0, 0],
+            weight_sems.at[1, 0, 0],
             {"sp": mate},
         )
 
@@ -339,11 +394,8 @@
         weight_over(index, flips[1]).wait_recv()
         weight_onward(index, flips[1]).start()
 
-    for index in range(EARLY):
-        weight_over(index, spot).start()
-    for half in range(2):
-        weight_mate(half, spot).start()
-
+
+    loaded(10, 11, 12)
     rims_do(range(3), "recv")
     columns = ((src_ref, src_halo, src_taps, xs), (wr_ref, wr_halo, wr_taps, wv), (rd_ref, rd_halo, rd_taps, rv))
     margin = CONV // 2
@@ -353,48 +405,14 @@
         for first in range(0, width, LANES):
             cols = slice(first, first + LANES)
             padded[8 : 8 + rows, :] = source[:, cols].astype(F32)
-            padded[0:8, :] = halo[0, TILE // 2 :, cols].astype(F32)
-            padded[8 + rows : 16 + rows, :] = halo[1, : TILE // 2, cols].astype(F32)
+            padded[0:8, :] = halo[0, :, cols].astype(F32)
+            padded[8 + rows : 16 + rows, :] = halo[1, :, cols].astype(F32)
             value = jnp.zeros((rows, LANES), F32)
             for k in range(CONV):
                 start = 8 - margin + k
                 value = value + padded[start : start + rows, :] * taps[k : k + 1, cols]
             target[:, cols] = silu(value).astype(BF16)
 
-    rims_do(range(3, 5), "recv")
-    sharing = q_ref.shape[1] // HEAD // kv_heads
-    above = iota((rows, rows), 1) >= iota((rows, rows), 0)
-    below = iota((rows, rows), 1) <= iota((rows, rows), 0)
-    ok_left = above & has_left
-    ok_right = below & has_right
-    scale = HEAD ** (-0.5)
-    for g in range(kv_heads):
-        cols = slice(g * HEAD, (g + 1) * HEAD)
-        keys = (k_halo[0, :, cols], turned[:, cols], k_halo[1, :, cols])
-        values = (v_halo[0, :, cols], v_ref[:, cols], v_halo[1, :, cols])
-        for j in range(sharing):
-            h = g * sharing + j
-            mine = slice(h * HEAD, (h + 1) * HEAD)
-            query = turn(q_ref[:, mine])
-            tiles = [dot_t(query, key) * scale for key in keys]
-            tiles[0] = jnp.where(ok_left, tiles[0], -jnp.inf)
-            tiles[2] = jnp.where(ok_right, tiles[2], -jnp.inf)
-            sink = sink_ref[h]
-            top = jnp.maximum(
-                jnp.max(
-                    jnp.maximum(jnp.maximum(tiles[0], tiles[1]), tiles[2]), axis=1, keepdims=True
-                ),
-                sink,
-            )
-            tiles = [jnp.exp(tile - top) for tile in tiles]
-            bottom = jnp.sum(tiles[0] + tiles[1] + tiles[2], axis=1, keepdims=True) + jnp.exp(
-                sink - top
-            )
-            found = jnp.zeros((rows, HEAD), F32)
-            for tile, value in zip(tiles, values):
-                found = found + dot((tile / bottom).astype(BF16), value)
-            acts[0, layer, :, mine] = found.astype(BF16)
-
     def own_copy(half, way_up):
         target = layer + (1 if way_up else -1)
         return sending(
@@ -404,6 +422,18 @@
             act_sems.at[1, half, layer],
             at_layer(target),
         )
+
+    part_wide = acts.shape[3]
+
+    def put(half, cols, value):
+        first = cols.start
+        while first < cols.stop:
+            part = first // part_wide
+            last = min(cols.stop, (part + 1) * part_wide)
+            acts[2 * half + part, layer, :, first - part * part_wide : last - part * part_wide] = value[
+                :, first - cols.start : last - cols.start
+            ].astype(BF16)
+            first = last
 
     can_up = layer < outer - 1
     can_down = layer > 0
@@ -434,8 +464,6 @@
             pl.when((target >= 0) & (target < outer))(lambda: copy.start())
 
         each(d, do)
-
-    own_start(0)
 
     groups = wr_ref.shape[1] // STATE
     wide = xs.shape[1]
@@ -468,6 +496,7 @@
         {"sp": mate},
     )
     swap.start()
+    weight_mate(spot).start()
 
     for flip, who in enumerate(flips):
         log_copy(flip, who, who).wait_recv()
@@ -543,18 +572,6 @@
             {"sp": mate},
         )
 
-    swap.wait_recv()
-    for c in range(CHUNKS):
-        part = slice(c * chunk, (c + 1) * chunk)
-        summed_state = (
-            mate_state[part, :].astype(F32) * dec_own + own_state[way, part, :]
-        )
-        total[part, :] = summed_state
-        total_out[part, :] = summed_state.astype(BF16)
-        over_copy(c).start()
-    for index in range(EARLY, 2 * PARTS):
-        weight_over(index, spot).start()
-
     run_at = square[0].T
     causal = iota((rows, rows), 1) <= iota((rows, rows), 0)
     diagonal = iota((rows, rows), 1) == iota((rows, rows), 0)
@@ -577,29 +594,104 @@
 
     for g in range(groups):
         within(g)
-    for index in range(EARLY):
-        pass_on(index)
+    swap.wait_recv()
+    for c in range(CHUNKS):
+        part = slice(c * chunk, (c + 1) * chunk)
+        summed_state = (
+            mate_state[part, :].astype(F32) * dec_own + own_state[way, part, :]
+        )
+        total[part, :] = summed_state
+        total_out[part, :] = summed_state.astype(BF16)
+        over_copy(c).start()
+
+    rims_do(range(3, 5), "recv")
+    loaded(14, 15)
+    sharing = q_ref.shape[1] // HEAD // kv_heads
+    stacked = (sharing * rows, rows)
+    query_at = lax.rem(iota(stacked, 0), rows)
+    above = iota(stacked, 1) >= query_at
+    below = iota(stacked, 1) <= query_at
+    ok_left = above & has_left
+    ok_right = below & has_right
+    scale = HEAD ** (-0.5)
+    for g in range(kv_heads):
+        cols = slice(g * HEAD, (g + 1) * HEAD)
+        keys = (k_halo[0, :, cols], turned[:, cols], k_halo[1, :, cols])
+        values = (v_halo[0, :, cols], v_ref[:, cols], v_halo[1, :, cols])
+        first = g * sharing
+        query = jnp.concatenate(
+            [turn(q_ref[:, h * HEAD : (h + 1) * HEAD]) for h in range(first, first + sharing)], axis=0
+        )
+        tiles = [dot_t(query, key) * scale for key in keys]
+        tiles[0] = jnp.where(ok_left, tiles[0], -jnp.inf)
+        tiles[2] = jnp.where(ok_right, tiles[2], -jnp.inf)
+        sink = jnp.concatenate(
+            [jnp.broadcast_to(sink_ref[:, h : h + 1], (rows, 1)) for h in range(first, first + sharing)],
+            axis=0,
+        )
+        top = jnp.maximum(
+            jnp.max(jnp.maximum(jnp.maximum(tiles[0], tiles[1]), tiles[2]), axis=1, keepdims=True),
+            sink,
+        )
+        tiles = [jnp.exp(tile - top) for tile in tiles]
+        bottom = jnp.sum(tiles[0] + tiles[1] + tiles[2], axis=1, keepdims=True) + jnp.exp(sink - top)
+        inverse = 1.0 / bottom
+        found = jnp.zeros((sharing * rows, HEAD), F32)
+        for tile, value in zip(tiles, values):
+            found = found + dot((tile * inverse).astype(BF16), value)
+        for j in range(sharing):
+            h = first + j
+            put(0, slice(h * HEAD, (h + 1) * HEAD), found[j * rows : (j + 1) * rows])
+    own_start(0)
+    own_start(1)
 
     for c in range(CHUNKS):
         part = slice(c * chunk, (c + 1) * chunk)
         over_copy(c).wait_recv()
-        theirs = partner_total[part, :].astype(F32)
-        level = theirs * from_partner + total[part, :] * from_mine
-        pl.when(has_before)(lambda: z_copy(c, after).wait_recv())
+        level = partner_total[part, :].astype(F32) * from_partner + total[part, :] * from_mine
+        total[part, :] = level
+
+        def first_out():
+            z_out[part, :] = level.astype(BF16)
+            z_copy(c, after).start()
+
+        pl.when(jnp.logical_not(has_before) & has_after)(first_out)
+    for index in range(PARTS):
+        weight_over(index, spot).start()
+    if outer > 1:
+        relay(0, 1)
+        relay(1, 1)
+    for c in range(CHUNKS):
+        part = slice(c * chunk, (c + 1) * chunk)
+
+        def next_out():
+            z_copy(c, after).wait_recv()
+
+            def send():
+                z_out[part, :] = (
+                    z_in[part, :].astype(F32) * dec_layer + total[part, :]
+                ).astype(BF16)
+                z_copy(c, after).start()
+
+            pl.when(has_after)(send)
+
+        pl.when(has_before)(next_out)
         entering = z_in[part, :].astype(F32)
-        z_out[part, :] = (entering * dec_layer + level).astype(BF16)
-        pl.when(has_after)(lambda: z_copy(c, after).start())
-        chip_in = entering * in_before + theirs * in_partner
+        chip_in = entering * in_before + partner_total[part, :].astype(F32) * in_partner
         chip_out[part, :] = chip_in.astype(BF16)
         down_copy(c).start()
         incoming[way, part, :] = (
             chip_in * dec_mate + mate_state[part, :].astype(F32)
         ).astype(BF16)
-    if outer > 1:
-        relay(0, 1)
+    for d in range(2, outer):
+        relay(0, d)
+        relay(1, d)
+        if d == 2:
+            break
     for c in range(CHUNKS):
         down_recv(c).wait_recv()
 
+    loaded(17, 18)
     for g in range(groups):
         cols = slice(g * group_wide, (g + 1) * group_wide)
         read = rv[:, g * STATE : (g + 1) * STATE]
@@ -609,90 +701,116 @@
         value = value * silu(gate_ref[:, cols].astype(F32))
         mean = jnp.sum(value * value, axis=1, keepdims=True) * (1.0 / group_wide)
         value = value * lax.rsqrt(mean + EPSILON) * gain_ref[:, cols]
-        acts[1, layer, :, cols] = value.astype(BF16)
-    own_start(1)
+        put(1, cols, value)
+    own_start(2)
+    own_start(3)
 
     share = rows // tps
 
     def multiply_first(block, sign):
         def body(slot, carry):
-            acc[block, slot] = dot(acts[0, block], weights[slot, 0])
+            acc[block, slot] = dot(acts[0, block], weights[slot, 0]) + dot(
+                acts[1, block], weights[slot, 1]
+            )
             return carry
 
         lax.fori_loop(0, CLIQUE, body, 0)
 
-    def piece_copy(block, other, slot):
-        return sending(
-            partial.at[block, other],
-            pieces.at[block, slot],
-            piece_sems.at[0, block, other],
-            piece_sems.at[1, block, slot],
+    def piece_copy(block, part, other, slot):
+        span = pl.ds(part * SPLIT, SPLIT)
+        return sending(
+            partial.at[block, other, span],
+            pieces.at[block, slot, span],
+            piece_sems.at[0, block, other, part],
+            piece_sems.at[1, block, slot, part],
             {"tp": other},
         )
 
     lanes = [lax.rem(lane + d, tps) for d in range(1, tps)]
+
+    def multiply_third(block, sign):
+        def body(slot, carry):
+            acc[block, slot] += dot(acts[2, block], weights[slot, 2])
+            return carry
+
+        lax.fori_loop(0, CLIQUE, body, 0)
 
     def multiply_second(block, sign):
         def body(slot, carry):
-            product = (acc[block, slot] + dot(acts[1, block], weights[slot, 1])).astype(BF16)
+            product = (acc[block, slot] + dot(acts[3, block], weights[slot, 3])).astype(BF16)
             for other in range(tps):
                 partial[block, other, slot] = product[other * share : (other + 1) * share]
             return carry
 
-        lax.fori_loop(0, CLIQUE, body, 0)
-        for other in lanes:
-            piece_copy(block, other, lane).start()
-
-    def out_copy(block, slot):
-        return sending(
-            summed.at[block],
-            landed.at[slot],
-            out_sems.at[0, block],
-            out_sems.at[1, slot],
+        for part in range(CLIQUE // SPLIT):
+            lax.fori_loop(part * SPLIT, (part + 1) * SPLIT, body, 0)
+            for other in lanes:
+                piece_copy(block, part, other, lane).start()
+
+    def out_copy(block, slot, part):
+        span = pl.ds(part * SPLIT, SPLIT)
+        return sending(
+            summed.at[block, span],
+            landed.at[slot, span],
+            out_sems.at[0, block, part],
+            out_sems.at[1, slot, part],
             at_layer(block),
         )
 
     def settle(block, sign):
-        result = partial[block, lane].astype(F32)
-        for other in lanes:
-            piece_copy(block, other, other).wait_recv()
-            result = result + pieces[block, other].astype(F32)
-        if sign:
-            summed[block] = result.astype(BF16)
-            out_copy(block, layer).start()
-        else:
-            landed[layer] = result.astype(BF16)
-
-    for index in range(EARLY, PARTS):
+        for part in range(CLIQUE // SPLIT):
+            span = slice(part * SPLIT, (part + 1) * SPLIT)
+            result = partial[block, lane, span].astype(F32)
+            for other in lanes:
+                piece_copy(block, part, other, other).wait_recv()
+                result = result + pieces[block, other, span].astype(F32)
+            if sign:
+                summed[block, span] = result.astype(BF16)
+                out_copy(block, layer, part).start()
+            else:
+                landed[layer, span] = result.astype(BF16)
+
+    weight_mate(flips[0]).wait_recv()
+    for index in range(2):
         pass_on(index)
-    weight_mate(0, flips[0]).wait_recv()
-    for index in range(PARTS):
+    for index in range(2):
         weight_onward(index, flips[2]).wait_recv()
     multiply_first(layer, 0)
-    for d in range(1, outer):
-        if d > 1:
+    if outer > 1:
+        each(1, multiply_first)
+    if outer > 1:
+        relay(2, 1)
+        relay(3, 1)
+    for d in range(2, outer):
+        if d > 2:
             relay(0, d)
+            relay(1, d)
         each(d, multiply_first)
-    for index in range(PARTS, 2 * PARTS):
+    for index in range(2, PARTS):
         pass_on(index)
-    weight_mate(1, flips[0]).wait_recv()
-    for index in range(PARTS, 2 * PARTS):
+    for index in range(2, PARTS):
         weight_onward(index, flips[2]).wait_recv()
+    multiply_third(layer, 0)
     multiply_second(layer, 0)
-    for d in range(1, outer):
-        relay(1, d)
+    if outer > 1:
+        each(1, multiply_third)
+        each(1, multiply_second)
+    for d in range(2, outer):
+        relay(2, d)
+        each(d, multiply_third)
+        relay(3, d)
         each(d, multiply_second)
-        if d == 1:
+        if d == 2:
             settle(layer, 0)
-        else:
-            each(d - 1, settle)
+        each(d - 1, settle)
+    if outer < 3:
+        settle(layer, 0)
     if outer > 1:
         each(outer - 1, settle)
-    else:
-        settle(layer, 0)
 
     def arrive(block, sign):
-        out_copy(block, block).wait_recv()
+        for part in range(CLIQUE // SPLIT):
+            out_copy(block, block, part).wait_recv()
 
     for d in range(1, outer):
         each(d, arrive)
@@ -705,11 +823,11 @@
     rims_do(range(5), "send")
     for flip, who in enumerate(flips):
         log_copy(flip, who, spot).wait_send()
-    for half in range(2):
-        weight_mate(half, spot).wait_send()
+    weight_mate(spot).wait_send()
+    for half in range(PARTS):
         pl.when(can_up)(lambda: own_copy(half, True).wait_send())
         pl.when(can_down)(lambda: own_copy(half, False).wait_send())
-    for index in range(2 * PARTS):
+    for index in range(PARTS):
         weight_over(index, spot).wait_send()
         weight_onward(index, flips[1]).wait_send()
     swap.wait_send()
@@ -720,18 +838,20 @@
 
     def gone(block, sign):
         target = layer - sign
-        for half in range(2):
+        for half in range(PARTS):
             pl.when((target >= 0) & (target < outer))(
                 lambda: far_copy(half, block, sign).wait_send()
             )
-        out_copy(block, layer).wait_send()
-        for other in lanes:
-            piece_copy(block, other, lane).wait_send()
+        for part in range(CLIQUE // SPLIT):
+            out_copy(block, layer, part).wait_send()
+            for other in lanes:
+                piece_copy(block, part, other, lane).wait_send()
 
     for d in range(1, outer):
         each(d, gone)
-    for other in lanes:
-        piece_copy(layer, other, lane).wait_send()
+    for part in range(CLIQUE // SPLIT):
+        for other in lanes:
+            piece_copy(layer, part, other, lane).wait_send()
 
 
 def local(
@@ -763,22 +883,36 @@
     width = final_mapping_matrix.shape[2]
     share = rows // tps
     halfway = HEAD // 2
-    spacing = ROTARY_BASE ** (-jnp.arange(halfway, dtype=F32) * 2.0 / HEAD)
-    places = (lax.axis_index("sp") * rows + jnp.arange(rows, dtype=jnp.int32)).astype(F32)
-    angles = places[:, None] * jnp.concatenate([spacing, spacing])[None, :]
-    sign = jnp.where(jnp.arange(HEAD) < halfway, -1.0, 1.0).astype(F32)
-    cosine = jnp.cos(angles)
-    sine = jnp.sin(angles) * sign[None, :]
-    vmem = pl.BlockSpec(memory_space=pltpu.VMEM)
+    spacing = ROTARY_BASE ** (-np.arange(halfway, dtype=np.float64) * 2.0 / HEAD)
+    spacing = np.concatenate([spacing, spacing])
+    angles = np.arange(rows, dtype=np.float64)[:, None] * spacing[None, :]
+    firsts = np.arange(count, dtype=np.float64)[:, None] * rows * spacing[None, :]
+    turns = np.stack([np.cos(firsts), np.sin(firsts)]).astype(np.float32)
     block = (CLIQUE, share, width)
     return pl.pallas_call(
         functools.partial(mixer_kernel, outer, tps),
         out_shape=jax.ShapeDtypeStruct((share, count * width), BF16),
-        in_specs=[vmem] * 13
-        + [pl.BlockSpec(memory_space=pltpu.SMEM), vmem, pl.BlockSpec(memory_space=pl.ANY)]
-        + [vmem] * 2,
-        out_specs=vmem,
+        in_specs=[pl.BlockSpec(memory_space=pl.ANY)] * 19,
+        out_specs=pl.BlockSpec(memory_space=pltpu.VMEM),
         scratch_shapes=[
+            pltpu.VMEM((rows, q_width), BF16),
+            pltpu.VMEM((rows, k_width), BF16),
+            pltpu.VMEM((rows, k_width), BF16),
+            pltpu.VMEM((rows, s_width), BF16),
+            pltpu.VMEM((rows, s_width), BF16),
+            pltpu.VMEM((rows, w_width), BF16),
+            pltpu.VMEM((rows, w_width), BF16),
+            pltpu.VMEM((CONV, s_width), BF16),
+            pltpu.VMEM((CONV, w_width), BF16),
+            pltpu.VMEM((CONV, w_width), BF16),
+            pltpu.VMEM((2, heads, rows), F32),
+            pltpu.VMEM((2, heads), F32),
+            pltpu.VMEM((2, heads, rows), F32),
+            pltpu.VMEM((1, q_width // HEAD), F32),
+            pltpu.VMEM((1, s_width), F32),
+            pltpu.VMEM((rows, HEAD), F32),
+            pltpu.VMEM((rows, HEAD), F32),
+            pltpu.VMEM((2, count, HEAD), F32),
             pltpu.VMEM((rows, k_width), BF16),
             pltpu.VMEM((2, rows, k_width), BF16),
             pltpu.VMEM((2, rows, k_width), BF16),
@@ -806,8 +940,8 @@
             pltpu.VMEM((STATE, s_width), BF16),
             pltpu.VMEM((2, STATE, s_width), BF16),
             pltpu.VMEM((rows, s_width), F32),
-            pltpu.VMEM((2, outer, rows, q_width), BF16),
-            pltpu.VMEM((CLIQUE,) + final_mapping_matrix.shape, BF16),
+            pltpu.VMEM((PARTS, outer, rows, q_width // 2), BF16),
+            pltpu.VMEM((CLIQUE, PARTS, q_width // 2, width), BF16),
             pltpu.VMEM((outer, CLIQUE, rows, width), F32),
             pltpu.VMEM((outer, tps) + block, BF16),
             pltpu.VMEM((outer, tps) + block, BF16),
@@ -815,13 +949,13 @@
             pltpu.VMEM((outer,) + block, BF16),
             pltpu.SemaphoreType.DMA((2, 2, 5)),
             pltpu.SemaphoreType.DMA((2, CLIQUE)),
-            pltpu.SemaphoreType.DMA((2, 3, 2 * PARTS)),
+            pltpu.SemaphoreType.DMA((2, 3, PARTS)),
             pltpu.SemaphoreType.DMA((2, 4, CHUNKS)),
-            pltpu.SemaphoreType.DMA((2, 2, outer)),
-            pltpu.SemaphoreType.DMA((2, 2)),
-            pltpu.SemaphoreType.DMA((2, outer, tps)),
-            pltpu.SemaphoreType.DMA((2, outer)),
-            pltpu.SemaphoreType.DMA,
+            pltpu.SemaphoreType.DMA((2, PARTS, outer)),
+            pltpu.SemaphoreType.DMA((PARTS, 2)),
+            pltpu.SemaphoreType.DMA((2, outer, tps, CLIQUE // SPLIT)),
+            pltpu.SemaphoreType.DMA((2, outer, CLIQUE // SPLIT)),
+            pltpu.SemaphoreType.DMA((19,)),
         ],
         compiler_params=pltpu.CompilerParams(collective_id=1, has_side_effects=True),
     )(
@@ -838,11 +972,12 @@
         raw_increment_lengths,
         logarithmic_fading_speeds,
         token_fading_spikes,
-        absorber_score_vector,
+        absorber_score_vector.reshape(1, q_width // HEAD),
         cluster_scaling_factor.reshape(1, s_width),
-        final_mapping_matrix,
-        cosine,
-        sine,
+        final_mapping_matrix.reshape(PARTS, q_width // 2, width),
+        np.cos(angles).astype(np.float32),
+        np.sin(angles).astype(np.float32),
+        turns,
     )
 
 

time: 86.1 us -> 73.1 us (0.85)
  Pallas kernels: 83 us -> 71 us
  other arithmetic: 1.06 us -> 0 us
    pallas_call x1, Pallas kernels: 83 us -> 71 us  [local(): pl.pallas_call(functools.partial(mixer_kernel, outer, tps), out_shape=jax...]
    mul x1 -> x0, other arithmetic: 0.97 us -> none  [local(): sine = jnp.sin(angles) * sign[None, :]]
where the time goes in v2:
time: 73.1 us; the launch traced here: 72.9 us
  Pallas kernels  71 us (97%)
  local copies, waits for them, and re-layouts  1.87 us (3%)
    pallas_call x1, Pallas kernels, local(): pl.pallas_call(functools.partial(mixer_kernel, outer, tps), out_shape=jax...  71 us
    unnamed x1, local copies, waits for them, and re-layouts  1.87 us

profile of v2, /device:TPU:0, one launch (start us, length us, event | category | flops | bytes accessed | tf_op | source)
XLA Modules:
  0.0 72.9 jit_solution(11539455062724831723)
XLA Ops:
  0.0 71.0 %shard_map.181 = bf16[64,4096]{1,0:T(8,128)(2,1)} custom-call(bf16[128,1024]{1,0:T(8,128)(2,1)} %q_hbm.1, bf16[128,512]{1,0:T(8,128)(2,1)} %k_hbm.1, bf16[128,512]{1,0:T(8,128)(2,1)} %v_hbm.1, bf16[128,1024]{1,0:T(8,128)(2,1)} %gate_hbm.1, bf16[128,1024]{1,0:T(8,128)(2,1)} %src_hbm.1, bf16[128,512]{1,0:T(8,128)(2,1)} %wr_hbm.1, bf16[128,512]{1,0:T(8,128)(2,1)} %rd_hbm.1, ...), custom_call_target="tpu_custom_call" | custom-call | tf_op jit(solution)/shard_map/pallas_call | solution.py:892
  71.0 1.9 %copy.21 = bf16[64,4096]{1,0:T(8,128)(2,1)} copy(bf16[64,4096]{1,0:T(8,128)(2,1)} %shard_map.181) | data formatting | bytes 1048576

commit v3 on v2

--- a/solution.py
+++ b/solution.py
@@ -134,6 +134,9 @@
     pieces,
     summed,
     landed,
+    spare,
+    first_out_sum,
+    first_in_sum,
     halo_sems,
     log_sems,
     weight_sems,
@@ -142,6 +145,8 @@
     own_sems,
     piece_sems,
     out_sems,
+    spare_sems,
+    first_sems,
     load_sems,
 ):
     count = outer * CLIQUE
@@ -167,6 +172,26 @@
     has_right = me < count - 1
     left = {"sp": me - 1}
     right = {"sp": me + 1}
+
+    lean = outer >= 4
+    low = (layer < 2).astype(jnp.int32)
+    buddy = low * (1 - layer) + (1 - low) * (2 * outer - 3 - layer)
+    giver = (layer == 0) | (layer == outer - 1)
+    taker = (layer == 1) | (layer == outer - 2)
+
+    def if_giver(do):
+        if lean:
+            pl.when(giver)(do)
+
+    def if_taker(do):
+        if lean:
+            pl.when(taker)(do)
+
+    def if_not_giver(do):
+        if lean:
+            pl.when(jnp.logical_not(giver))(do)
+        else:
+            do()
 
     def at_layer(other):
         return {"sp": other * CLIQUE + spot}
@@ -438,9 +463,15 @@
     can_up = layer < outer - 1
     can_down = layer > 0
 
+    def own_goes(half, way_up):
+        can = can_up if way_up else can_down
+        if lean and half >= 2:
+            can = can & jnp.logical_not(taker & (buddy == layer + (1 if way_up else -1)))
+        return can
+
     def own_start(half):
-        pl.when(can_up)(lambda: own_copy(half, True).start())
-        pl.when(can_down)(lambda: own_copy(half, False).start())
+        pl.when(own_goes(half, True))(lambda: own_copy(half, True).start())
+        pl.when(own_goes(half, False))(lambda: own_copy(half, False).start())
 
     def far_copy(half, block, sign):
         return sending(
@@ -463,7 +494,10 @@
             target = layer - sign
             pl.when((target >= 0) & (target < outer))(lambda: copy.start())
 
-        each(d, do)
+        if half >= 2 and d == 1:
+            if_not_giver(lambda: each(d, do))
+        else:
+            each(d, do)
 
     groups = wr_ref.shape[1] // STATE
     wide = xs.shape[1]
@@ -658,6 +692,30 @@
         pl.when(jnp.logical_not(has_before) & has_after)(first_out)
     for index in range(PARTS):
         weight_over(index, spot).start()
+    def spare_in(index):
+        return sending(
+            weights.at[spot, 2 + index],
+            spare.at[spot, index],
+            spare_sems.at[0, 0, index],
+            spare_sems.at[1, 0, index],
+            at_layer(buddy),
+        )
+
+    def spare_on(kind, index, slot, who):
+        return sending(
+            spare.at[slot, index],
+            spare.at[slot, index],
+            spare_sems.at[0, kind, index],
+            spare_sems.at[1, kind, index],
+            {"sp": who},
+        )
+
+    def give_weights():
+        for index in range(2):
+            spare_in(index).start()
+
+    if_giver(give_weights)
+
     if outer > 1:
         relay(0, 1)
         relay(1, 1)
@@ -703,7 +761,6 @@
         value = value * lax.rsqrt(mean + EPSILON) * gain_ref[:, cols]
         put(1, cols, value)
     own_start(2)
-    own_start(3)
 
     share = rows // tps
 
@@ -776,44 +833,120 @@
     for index in range(2):
         weight_onward(index, flips[2]).wait_recv()
     multiply_first(layer, 0)
+    own_start(3)
     if outer > 1:
         each(1, multiply_first)
+
+    first_copy = sending(
+        first_out_sum, first_in_sum, first_sems.at[0], first_sems.at[1], at_layer(buddy)
+    )
+
+    def give_first():
+        def body(slot, carry):
+            first_out_sum[slot] = acc[buddy, slot].astype(BF16)
+            return carry
+
+        lax.fori_loop(0, CLIQUE, body, 0)
+        first_copy.start()
+
+    if_giver(give_first)
     if outer > 1:
         relay(2, 1)
-        relay(3, 1)
     for d in range(2, outer):
         if d > 2:
             relay(0, d)
             relay(1, d)
         each(d, multiply_first)
+    if outer > 1:
+        relay(3, 1)
+    if outer > 2:
+        relay(2, 2)
     for index in range(2, PARTS):
         pass_on(index)
     for index in range(2, PARTS):
         weight_onward(index, flips[2]).wait_recv()
+
+    def spread_spare():
+        for index in range(2):
+            spare_in(index).wait_recv()
+            spare_on(2, index, spot, partner).start()
+            spare_on(1, index, spot, mate).start()
+
+    if_taker(spread_spare)
+    def nearest():
+        each(1, multiply_third)
+        each(1, multiply_second)
+
+    if outer > 1:
+        if_not_giver(nearest)
+    if outer > 2:
+        relay(3, 2)
+    if outer > 2:
+        each(2, multiply_third)
+        each(2, multiply_second)
     multiply_third(layer, 0)
     multiply_second(layer, 0)
     if outer > 1:
-        each(1, multiply_third)
-        each(1, multiply_second)
-    for d in range(2, outer):
+        if_not_giver(lambda: each(1, settle))
+    for d in range(3, outer):
         relay(2, d)
         each(d, multiply_third)
         relay(3, d)
         each(d, multiply_second)
-        if d == 2:
-            settle(layer, 0)
         each(d - 1, settle)
-    if outer < 3:
-        settle(layer, 0)
-    if outer > 1:
+
+    def extra_block():
+        for index in range(2):
+            spare_on(2, index, flips[1], partner).wait_recv()
+            spare_on(3, index, flips[1], mate).start()
+        first_copy.wait_recv()
+        for index in range(2):
+            spare_on(1, index, flips[0], mate).wait_recv()
+        for index in range(2):
+            spare_on(3, index, flips[2], mate).wait_recv()
+
+        def body(slot, carry):
+            product = (
+                first_in_sum[slot].astype(F32)
+                + dot(acts[2, layer], spare[slot, 0])
+                + dot(acts[3, layer], spare[slot, 1])
+            ).astype(BF16)
+            for other in range(tps):
+                partial[outer, other, slot] = product[other * share : (other + 1) * share]
+            return carry
+
+        for part in range(CLIQUE // SPLIT):
+            lax.fori_loop(part * SPLIT, (part + 1) * SPLIT, body, 0)
+            for other in lanes:
+                piece_copy(outer, part, other, lane).start()
+
+    def extra_settle():
+        for part in range(CLIQUE // SPLIT):
+            span = slice(part * SPLIT, (part + 1) * SPLIT)
+            result = partial[outer, lane, span].astype(F32)
+            for other in lanes:
+                piece_copy(outer, part, other, other).wait_recv()
+                result = result + pieces[outer, other, span].astype(F32)
+            landed[buddy, span] = result.astype(BF16)
+
+    if_taker(extra_block)
+    if outer > 2:
         each(outer - 1, settle)
+    settle(layer, 0)
+    if_taker(extra_settle)
 
     def arrive(block, sign):
         for part in range(CLIQUE // SPLIT):
             out_copy(block, block, part).wait_recv()
 
+    def arrive_near(block, sign):
+        if lean:
+            pl.when(jnp.logical_not(taker & (block == buddy)))(lambda: arrive(block, sign))
+        else:
+            arrive(block, sign)
+
     for d in range(1, outer):
-        each(d, arrive)
+        each(d, arrive_near if d == 1 else arrive)
     width = landed.shape[3]
     for other in range(outer):
         for slot in range(CLIQUE):
@@ -825,8 +958,8 @@
         log_copy(flip, who, spot).wait_send()
     weight_mate(spot).wait_send()
     for half in range(PARTS):
-        pl.when(can_up)(lambda: own_copy(half, True).wait_send())
-        pl.when(can_down)(lambda: own_copy(half, False).wait_send())
+        pl.when(own_goes(half, True))(lambda: own_copy(half, True).wait_send())
+        pl.when(own_goes(half, False))(lambda: own_copy(half, False).wait_send())
     for index in range(PARTS):
         weight_over(index, spot).wait_send()
         weight_onward(index, flips[1]).wait_send()
@@ -847,7 +980,25 @@
             for other in lanes:
                 piece_copy(block, part, other, lane).wait_send()
 
-    for d in range(1, outer):
+    def given():
+        for index in range(2):
+            spare_in(index).wait_send()
+        first_copy.wait_send()
+
+    def taken():
+        for index in range(2):
+            spare_on(1, index, spot, mate).wait_send()
+            spare_on(2, index, spot, partner).wait_send()
+            spare_on(3, index, flips[1], mate).wait_send()
+        for part in range(CLIQUE // SPLIT):
+            for other in lanes:
+                piece_copy(outer, part, other, lane).wait_send()
+
+    if_giver(given)
+    if_taker(taken)
+    if outer > 1:
+        if_not_giver(lambda: each(1, gone))
+    for d in range(2, outer):
         each(d, gone)
     for part in range(CLIQUE // SPLIT):
         for other in lanes:
@@ -943,18 +1094,23 @@
             pltpu.VMEM((PARTS, outer, rows, q_width // 2), BF16),
             pltpu.VMEM((CLIQUE, PARTS, q_width // 2, width), BF16),
             pltpu.VMEM((outer, CLIQUE, rows, width), F32),
-            pltpu.VMEM((outer, tps) + block, BF16),
-            pltpu.VMEM((outer, tps) + block, BF16),
+            pltpu.VMEM((outer + 1, tps) + block, BF16),
+            pltpu.VMEM((outer + 1, tps) + block, BF16),
             pltpu.VMEM((outer,) + block, BF16),
             pltpu.VMEM((outer,) + block, BF16),
+            pltpu.VMEM((CLIQUE, 2, q_width // 2, width), BF16),
+            pltpu.VMEM((CLIQUE, rows, width), BF16),
+            pltpu.VMEM((CLIQUE, rows, width), BF16),
             pltpu.SemaphoreType.DMA((2, 2, 5)),
             pltpu.SemaphoreType.DMA((2, CLIQUE)),
             pltpu.SemaphoreType.DMA((2, 3, PARTS)),
             pltpu.SemaphoreType.DMA((2, 4, CHUNKS)),
             pltpu.SemaphoreType.DMA((2, PARTS, outer)),
             pltpu.SemaphoreType.DMA((PARTS, 2)),
-            pltpu.SemaphoreType.DMA((2, outer, tps, CLIQUE // SPLIT)),
+            pltpu.SemaphoreType.DMA((2, outer + 1, tps, CLIQUE // SPLIT)),
             pltpu.SemaphoreType.DMA((2, outer, CLIQUE // SPLIT)),
+            pltpu.SemaphoreType.DMA((2, 4, 2)),
+            pltpu.SemaphoreType.DMA((2,)),
             pltpu.SemaphoreType.DMA((19,)),
         ],
         compiler_params=pltpu.CompilerParams(collective_id=1, has_side_effects=True),

time: 73.1 us -> 72.6 us (level)
  no operation moved by 1% of the time
where the time goes in v3:
time: 72.6 us; the launch traced here: 72.5 us
  Pallas kernels  70.6 us (97%)
  local copies, waits for them, and re-layouts  1.87 us (3%)
    pallas_call x1, Pallas kernels, local(): pl.pallas_call(functools.partial(mixer_kernel, outer, tps), out_shape=jax...  70.6 us
    unnamed x1, local copies, waits for them, and re-layouts  1.87 us

profile of v3, /device:TPU:0, one launch (start us, length us, event | category | flops | bytes accessed | tf_op | source)
XLA Modules:
  0.0 72.5 jit_solution(14192137973556584776)
XLA Ops:
  0.0 70.6 %shard_map.181 = bf16[64,4096]{1,0:T(8,128)(2,1)} custom-call(bf16[128,1024]{1,0:T(8,128)(2,1)} %q_hbm.1, bf16[128,512]{1,0:T(8,128)(2,1)} %k_hbm.1, bf16[128,512]{1,0:T(8,128)(2,1)} %v_hbm.1, bf16[128,1024]{1,0:T(8,128)(2,1)} %gate_hbm.1, bf16[128,1024]{1,0:T(8,128)(2,1)} %src_hbm.1, bf16[128,512]{1,0:T(8,128)(2,1)} %wr_hbm.1, bf16[128,512]{1,0:T(8,128)(2,1)} %rd_hbm.1, ...), custom_call_target="tpu_custom_call" | custom-call | tf_op jit(solution)/shard_map/pallas_call | solution.py:1043
  70.6 1.9 %copy.21 = bf16[64,4096]{1,0:T(8,128)(2,1)} copy(bf16[64,4096]{1,0:T(8,128)(2,1)} %shard_map.181) | data formatting | bytes 1048576

commit v4 on v3

--- a/solution.py
+++ b/solution.py
@@ -677,7 +677,6 @@
             h = first + j
             put(0, slice(h * HEAD, (h + 1) * HEAD), found[j * rows : (j + 1) * rows])
     own_start(0)
-    own_start(1)
 
     for c in range(CHUNKS):
         part = slice(c * chunk, (c + 1) * chunk)
@@ -690,6 +689,7 @@
             z_copy(c, after).start()
 
         pl.when(jnp.logical_not(has_before) & has_after)(first_out)
+    own_start(1)
     for index in range(PARTS):
         weight_over(index, spot).start()
     def spare_in(index):
@@ -718,7 +718,6 @@
 
     if outer > 1:
         relay(0, 1)
-        relay(1, 1)
     for c in range(CHUNKS):
         part = slice(c * chunk, (c + 1) * chunk)
 
@@ -741,11 +740,10 @@
         incoming[way, part, :] = (
             chip_in * dec_mate + mate_state[part, :].astype(F32)
         ).astype(BF16)
-    for d in range(2, outer):
-        relay(0, d)
-        relay(1, d)
-        if d == 2:
-            break
+    if outer > 1:
+        relay(1, 1)
+    if outer > 2:
+        relay(0, 2)
     for c in range(CHUNKS):
         down_recv(c).wait_recv()
 
@@ -827,6 +825,8 @@
             else:
                 landed[layer, span] = result.astype(BF16)
 
+    if outer > 2:
+        relay(1, 2)
     weight_mate(flips[0]).wait_recv()
     for index in range(2):
         pass_on(index)

time: 72.6 us -> 70.2 us (0.967)
  Pallas kernels: 70.6 us -> 67.7 us
    pallas_call x1, Pallas kernels: 70.6 us -> 67.7 us  [local(): pl.pallas_call(functools.partial(mixer_kernel, outer, tps), out_shape=jax...]
where the time goes in v4:
time: 70.2 us; the launch traced here: 69.6 us
  Pallas kernels  67.7 us (96%)
  local copies, waits for them, and re-layouts  1.87 us (3%)
    pallas_call x1, Pallas kernels, local(): pl.pallas_call(functools.partial(mixer_kernel, outer, tps), out_shape=jax...  67.7 us
    unnamed x1, local copies, waits for them, and re-layouts  1.87 us

profile of v4, /device:TPU:0, one launch (start us, length us, event | category | flops | bytes accessed | tf_op | source)
XLA Modules:
  0.0 69.6 jit_solution(17459783110768242102)
XLA Ops:
  0.0 67.7 %shard_map.181 = bf16[64,4096]{1,0:T(8,128)(2,1)} custom-call(bf16[128,1024]{1,0:T(8,128)(2,1)} %q_hbm.1, bf16[128,512]{1,0:T(8,128)(2,1)} %k_hbm.1, bf16[128,512]{1,0:T(8,128)(2,1)} %v_hbm.1, bf16[128,1024]{1,0:T(8,128)(2,1)} %gate_hbm.1, bf16[128,1024]{1,0:T(8,128)(2,1)} %src_hbm.1, bf16[128,512]{1,0:T(8,128)(2,1)} %wr_hbm.1, bf16[128,512]{1,0:T(8,128)(2,1)} %rd_hbm.1, ...), custom_call_target="tpu_custom_call" | custom-call | tf_op jit(solution)/shard_map/pallas_call | solution.py:1043
  67.7 1.9 %copy.21 = bf16[64,4096]{1,0:T(8,128)(2,1)} copy(bf16[64,4096]{1,0:T(8,128)(2,1)} %shard_map.181) | data formatting | bytes 1048576
